TPU v7x, 32 devices: a whole 2x2x4 slice. The times are simulated.
32 devices in a mesh: ep: 8 (over z, y), tp: 4 (over x, core).
Axes of the slice: x: 2, y: 2, z: 4, core: 2. Of those that a mesh axis runs over, the one named last changes fastest.
Arguments:
- queries: bfloat16 [4096, 1024], P('ep', 'tp'), may hold values from -8 to 8
- key_rows: bfloat16 [4096, 1024], P('ep', 'tp'), may hold values from -8 to 8
- value_rows: bfloat16 [4096, 1024], P('ep', 'tp'), may hold values from -6 to 6
- lambdas: float32 [8], P('tp'), may hold values from 0.3 to 0.8
- head_gain: float32 [128], replicated, may hold values from 0.1 to 1.9
- out_weight: bfloat16 [1024, 2048], P('tp'), may hold values from -0.1875 to 0.1875
- moe_input: bfloat16 [4096, 2048], P(('ep', 'tp')), may hold values from -400 to 400
- moe_gain: float32 [2048], replicated, may hold values from 0.1 to 1.9
- routes: int32 [4096, 2], P(('ep', 'tp')), may hold values from 0 to 7, all different within a row; in each aligned block of 128 rows (0 to 127, 128 to 255, ...) at most 40 rows name the same one
- route_logits: float32 [4096, 2], P(('ep', 'tp')), may hold values from -6 to 6
- expert_gate: bfloat16 [8, 2048, 3584], P('ep', None, 'tp'), may hold values from -0.125 to 0.125
- expert_up: bfloat16 [8, 2048, 3584], P('ep', None, 'tp'), may hold values from -0.125 to 0.125
- expert_down: bfloat16 [8, 3584, 2048], P('ep', 'tp'), may hold values from -0.09375 to 0.09375
Outputs:
- mixer_out: bfloat16 [4096, 2048], P(('ep', 'tp'))
- expert_out: bfloat16 [4096, 2048], P(('ep', 'tp'))
Inputs may be any that keep to these rules, and one draw needn't show every extreme that they name: `routes`: each token names 2 different experts. Among the tokens of one device no expert is named more than 40 times, and in every draw some expert is named exactly 40 times by the tokens of some device.
All inputs are finite; a program needn't handle non-finite values.
Results may differ from a plain program's by a relative error of at most 0.014.
Values may be sent and summed in bfloat16 or wider, within the bound.
No kernel may reach another device: no remote copies, remote signals or barrier semaphores. Data moves between devices by JAX's collectives and lax.ppermute only.
A program may use at most 128 MiB of HBM per device.

v0:
```python
import functools

import jax
import jax.numpy as jnp
from jax import lax
from jax.experimental import pallas as pl
from jax.experimental.pallas import tpu as pltpu
from jax.sharding import PartitionSpec as P


epsilon = 1e-06
init_lambda = 0.2
small_vmem = 12 * 1024 * 1024
expert_vmem = 24 * 1024 * 1024
attention_vmem = 32 * 1024 * 1024


whole_vmem = pl.BlockSpec(memory_space=pltpu.VMEM)


def capacity(tokens, top_count, experts):
    return max(2, (top_count * tokens * 5 + 4 * experts - 1) // (4 * experts))


def swap(array, axis, mask):
    size = lax.axis_size(axis)
    return lax.ppermute(array, axis, [(i, i ^ mask) for i in range(size)])


def dispatch_kernel(cap, x_ref, gain_ref, hops_ref, ranks_ref, *blocks):
    tokens, _ = x_ref.shape
    rows = x_ref[...].astype(jnp.float32)
    mean_square = jnp.mean(rows * rows, axis=-1, keepdims=True)
    normed = (rows * lax.rsqrt(mean_square + epsilon) * gain_ref[...]).astype(jnp.bfloat16)
    count = len(blocks)
    top = hops_ref.shape[0]
    earlier = lax.broadcasted_iota(jnp.int32, (tokens, tokens), 0)
    later = lax.broadcasted_iota(jnp.int32, (tokens, tokens), 1)
    before = (earlier < later).astype(jnp.float32).astype(jnp.bfloat16)
    hop_ids = lax.broadcasted_iota(jnp.int32, (count, tokens), 0)
    base = jnp.zeros((count, 1), jnp.float32)
    ranks = []
    for j in range(top):
        chosen = (hops_ref[j : j + 1, :] == hop_ids).astype(jnp.float32)
        prefix = jnp.dot(chosen.astype(jnp.bfloat16), before, preferred_element_type=jnp.float32)
        rank = jnp.sum(chosen * (prefix + base), axis=0, keepdims=True)
        base = base + jnp.sum(chosen, axis=1, keepdims=True)
        ranks.append(rank.astype(jnp.int32))
        ranks_ref[j : j + 1, :] = ranks[-1]
    places = lax.broadcasted_iota(jnp.int32, (cap, tokens), 0)
    picks = []
    for k in range(count):
        picked = jnp.zeros((cap, tokens), jnp.float32)
        for j in range(top):
            hit = (hops_ref[j : j + 1, :] == k) & (ranks[j] == places)
            picked = picked + hit.astype(jnp.float32)
        picks.append(picked)
    picks = jnp.concatenate(picks, axis=0).astype(jnp.bfloat16)
    rows = jnp.dot(picks, normed, preferred_element_type=jnp.float32)
    for k, block in enumerate(blocks):
        block[...] = rows[k * cap : (k + 1) * cap].astype(jnp.bfloat16)


def dispatch(moe_input, moe_gain, hops, cap, count):
    tokens, width = moe_input.shape
    shapes = [jax.ShapeDtypeStruct(hops.shape, jnp.int32)]
    shapes += [jax.ShapeDtypeStruct((cap, width), jnp.bfloat16)] * count
    out = pl.pallas_call(
        functools.partial(dispatch_kernel, cap),
        out_shape=shapes,
        in_specs=[whole_vmem] * 3,
        out_specs=[whole_vmem] * len(shapes),
        cost_estimate=pl.CostEstimate(flops=2 * cap * count * tokens * width, bytes_accessed=4 * tokens * width, transcendentals=0),
        compiler_params=pltpu.CompilerParams(vmem_limit_bytes=small_vmem),
        name="dispatch",
    )(moe_input, moe_gain.reshape(1, -1), hops)
    return out[0], list(out[1:])


def window_kernel(ranks_ref, gate_ref, up_ref, down_ref, out_ref):
    out_ref[...] = ranks_ref[...]


def window(ranks, *weights):
    return pl.pallas_call(
        window_kernel,
        out_shape=jax.ShapeDtypeStruct(ranks.shape, ranks.dtype),
        in_specs=[whole_vmem] * (1 + len(weights)),
        out_specs=whole_vmem,
        compiler_params=pltpu.CompilerParams(vmem_limit_bytes=small_vmem),
        cost_estimate=pl.CostEstimate(flops=1, bytes_accessed=4 * ranks.size, transcendentals=0),
        name="window",
    )(ranks, *weights)


def combine_kernel(hops_ref, ranks_ref, logits_ref, *refs):
    blocks, out_ref = refs[:-1], refs[-1]
    top, tokens = hops_ref.shape
    cap = blocks[0].shape[0]
    logits = logits_ref[...]
    peak = jnp.max(logits, axis=0, keepdims=True)
    raised = jnp.exp(logits - peak)
    gates = raised / jnp.sum(raised, axis=0, keepdims=True)
    places = lax.broadcasted_iota(jnp.int32, (cap, tokens), 0)
    parts = []
    for k in range(len(blocks)):
        weight = jnp.zeros((cap, tokens), jnp.float32)
        for j in range(top):
            hit = (hops_ref[j : j + 1, :] == k) & (ranks_ref[j : j + 1, :] == places)
            weight = weight + jnp.where(hit, gates[j : j + 1, :], 0.0)
        parts.append(weight)
    weights = jnp.concatenate(parts, axis=0)
    high = weights.astype(jnp.bfloat16)
    low = (weights - high.astype(jnp.float32)).astype(jnp.bfloat16)
    rows = jnp.concatenate([block[...] for block in blocks], axis=0)
    both = lax.dot_general(
        jnp.concatenate([high, low], axis=1),
        rows,
        (((0,), (0,)), ((), ())),
        preferred_element_type=jnp.float32,
    )
    out_ref[...] = (both[:tokens] + both[tokens:]).astype(jnp.bfloat16)


def combine(hops, ranks, logits, blocks):
    tokens, width = hops.shape[1], blocks[0].shape[1]
    return pl.pallas_call(
        combine_kernel,
        out_shape=jax.ShapeDtypeStruct((tokens, width), jnp.bfloat16),
        in_specs=[whole_vmem] * (3 + len(blocks)),
        out_specs=whole_vmem,
        cost_estimate=pl.CostEstimate(flops=4 * tokens * width * len(blocks) * blocks[0].shape[0], bytes_accessed=4 * tokens * width, transcendentals=0),
        compiler_params=pltpu.CompilerParams(vmem_limit_bytes=small_vmem),
        name="combine",
    )(hops, ranks, logits, *blocks)


def expert_kernel(count, *refs):
    inputs = refs[:count]
    gate_ref, up_ref, down_ref = refs[count : count + 3]
    outputs = refs[count + 3 : -1]
    hidden_ref = refs[-1]
    _, width = inputs[0].shape
    tile, wide = 128, min(512, width)
    order = list(range(0, count, 2)) + list(range(1, count, 2))

    def hidden_step(step, carry):
        at = pl.ds(pl.multiple_of(step * tile, tile), tile)
        x = jnp.concatenate([inputs[i][...] for i in order], axis=0)
        both = jnp.concatenate([gate_ref[:, at], up_ref[:, at]], axis=1)
        product = jnp.dot(x, both, preferred_element_type=jnp.float32)
        gate_part, up_part = product[:, :tile], product[:, tile:]
        hidden = gate_part / (1.0 + jnp.exp(-gate_part)) * up_part
        hidden_ref[:, at] = hidden.astype(jnp.bfloat16)
        return carry

    def down_step(step, carry):
        at = pl.ds(pl.multiple_of(step * wide, wide), wide)
        product = jnp.dot(hidden_ref[...], down_ref[:, at], preferred_element_type=jnp.float32)
        first = 0
        for ref in outputs:
            ref[:, at] = product[first : first + ref.shape[0]].astype(jnp.bfloat16)
            first += ref.shape[0]
        return carry

    lax.fori_loop(0, gate_ref.shape[1] // tile, hidden_step, 0)
    lax.fori_loop(0, width // wide, down_step, 0)


def expert(blocks, gate, up, down):
    count = len(blocks)
    rows, width = blocks[0].shape
    units = gate.shape[1]
    stay = count - count // 2
    shapes = [jax.ShapeDtypeStruct((rows, width), jnp.bfloat16)] * stay
    shapes += [jax.ShapeDtypeStruct((rows * (count // 2), width), jnp.bfloat16)]
    return pl.pallas_call(
        functools.partial(expert_kernel, count),
        out_shape=shapes,
        in_specs=[whole_vmem] * (count + 3),
        out_specs=[whole_vmem] * len(shapes),
        scratch_shapes=[pltpu.VMEM((count * rows, units), jnp.bfloat16)],
        compiler_params=pltpu.CompilerParams(vmem_limit_bytes=expert_vmem),
        cost_estimate=pl.CostEstimate(
            flops=6 * count * rows * width * units,
            bytes_accessed=6 * width * units + 4 * count * rows * width,
            transcendentals=count * rows * units,
        ),
    )(*blocks, gate, up, down)


def attention_kernel(heads, head_size, value_size, rows, count, mine_ref, lam_ref, gain_ref, q_ref, *refs):
    blocks, out_ref = refs[:count], refs[count]
    value_ref, score_a, score_b, peak_a, peak_b = refs[count + 1 :]
    tiles = q_ref.shape[0] // rows
    keys = blocks[0].shape[0]
    pair = 2 * head_size
    scale = head_size ** (-0.5)
    lanes = lax.broadcasted_iota(jnp.int32, (rows, pair), 1)

    for head in range(heads):
        lam = lam_ref[mine_ref[0] * heads + head]
        first_value = heads * pair + head * value_size

        for index, block in enumerate(blocks):
            at = slice(index * keys, (index + 1) * keys)
            value_ref[at, :value_size] = block[:, first_value : first_value + value_size]
            value_ref[at, value_size:] = jnp.ones((keys, value_size), jnp.bfloat16)

        def step(following, score_to, peak_to, current, score_from, peak_from):
            at = pl.ds(pl.multiple_of(following * rows, rows), rows)
            q = q_ref[at, head * pair : (head + 1) * pair].astype(jnp.float32) * scale
            q = jnp.concatenate(
                [jnp.where(lanes < head_size, q, 0.0), jnp.where(lanes < head_size, 0.0, q)], axis=0
            ).astype(jnp.bfloat16)
            peak = jnp.full((2 * rows, 128), -jnp.inf, jnp.float32)
            if current is not None:
                maxima = jnp.concatenate([peak_from[...]] * (keys // 128), axis=1)
                total = jnp.zeros((2 * rows, 2 * value_size), jnp.float32)
            for index, block in enumerate(blocks):
                columns = slice(index * keys, (index + 1) * keys)
                scores = lax.dot_general(
                    q,
                    block[:, head * pair : (head + 1) * pair],
                    (((1,), (1,)), ((), ())),
                    preferred_element_type=jnp.float32,
                )
                score_to[:, columns] = scores
                for part in range(keys // 128):
                    peak = jnp.maximum(peak, scores[:, part * 128 : (part + 1) * 128])
                if current is not None:
                    weights = jnp.exp(score_from[:, columns] - maxima)
                    total = total + jnp.dot(
                        weights.astype(jnp.bfloat16),
                        value_ref[columns, :],
                        preferred_element_type=jnp.float32,
                    )
            peak_to[...] = jnp.broadcast_to(jnp.max(peak, axis=1, keepdims=True), peak.shape)
            if current is not None:
                maps = total[:, :value_size] / total[:, value_size:]
                head_out = maps[:rows] - lam * maps[rows:]
                mean_square = jnp.mean(head_out * head_out, axis=-1, keepdims=True)
                normal = head_out * lax.rsqrt(mean_square + epsilon) * gain_ref[...] * (1.0 - init_lambda)
                out_at = pl.ds(pl.multiple_of(current * rows, rows), rows)
                out_ref[out_at, head * value_size : (head + 1) * value_size] = normal.astype(jnp.bfloat16)

        step(0, score_a, peak_a, None, None, None)

        def two_tiles(i, carry):
            step(2 * i + 1, score_b, peak_b, 2 * i, score_a, peak_a)
            step(jnp.minimum(2 * i + 2, tiles - 1), score_a, peak_a, 2 * i + 1, score_b, peak_b)
            return carry

        lax.fori_loop(0, tiles // 2, two_tiles, 0)


def attention(mine, lam, gain, q, blocks, heads):
    value_size = gain.shape[0]
    head_size = q.shape[1] // (2 * heads)
    queries = q.shape[0]
    keys = blocks[0].shape[0]
    total_keys = keys * len(blocks)
    rows = min(256, queries // 2)
    while rows > 16 and 8 * rows * total_keys > 2**23:
        rows //= 2
    smem = pl.BlockSpec(memory_space=pltpu.SMEM)
    return pl.pallas_call(
        functools.partial(attention_kernel, heads, head_size, value_size, rows, len(blocks)),
        out_shape=jax.ShapeDtypeStruct((queries, heads * value_size), jnp.bfloat16),
        in_specs=[smem, smem] + [whole_vmem] * (2 + len(blocks)),
        out_specs=whole_vmem,
        scratch_shapes=[pltpu.VMEM((total_keys, 2 * value_size), jnp.bfloat16)]
        + [pltpu.VMEM((2 * rows, total_keys), jnp.float32)] * 2
        + [pltpu.VMEM((2 * rows, 128), jnp.float32)] * 2,
        compiler_params=pltpu.CompilerParams(vmem_limit_bytes=attention_vmem),
        cost_estimate=pl.CostEstimate(
            flops=heads * queries * total_keys * 2 * 2 * (head_size + value_size) * 2,
            bytes_accessed=2 * total_keys * heads * (2 * head_size + value_size),
            transcendentals=2 * heads * queries * total_keys,
        ),
    )(mine.reshape(1), lam, gain.reshape(1, -1), q, *blocks)


def mixer_kernel(count, mine_ref, *refs):
    columns, weights, out_ref = refs[:count], refs[count:-1], refs[-1]
    half = columns[0].shape[1] // 2
    first = mine_ref[0] == 0
    ordered = []
    for ref in columns:
        kept, other = ref[:, :half], ref[:, half:]
        ordered += [jnp.where(first, kept, other), jnp.where(first, other, kept)]
    out_ref[...] = jnp.dot(
        jnp.concatenate(ordered, axis=1),
        jnp.concatenate([ref[...] for ref in weights], axis=0),
        preferred_element_type=jnp.float32,
    ).astype(jnp.bfloat16)


def mixer(mine, columns, weights):
    rows, width = columns[0].shape[0], weights[0].shape[1]
    return pl.pallas_call(
        functools.partial(mixer_kernel, len(columns)),
        out_shape=jax.ShapeDtypeStruct((rows, width), jnp.bfloat16),
        in_specs=[pl.BlockSpec(memory_space=pltpu.SMEM)] + [whole_vmem] * (len(columns) + len(weights)),
        out_specs=whole_vmem,
        compiler_params=pltpu.CompilerParams(vmem_limit_bytes=expert_vmem),
        cost_estimate=pl.CostEstimate(
            flops=2 * rows * width * sum(w.shape[0] for w in weights),
            bytes_accessed=2 * width * sum(w.shape[0] for w in weights),
            transcendentals=0,
        ),
        name="mixer",
    )(mine.reshape(1), *columns, *weights)


def gather_all(block, axis, size):
    held = {0: block}
    bit = size // 2
    while bit:
        for index in list(held):
            held[index ^ bit] = swap(held[index], axis, bit)
        bit //= 2
    return [held[i] for i in range(size)]


def scatter_tp(stay, sent):
    came = swap(sent, "tp", 1)
    rows = stay[0].shape[0]
    held = {}
    for i in reversed(range(len(stay))):
        held[2 * i] = add_rounded(stay[i], came[i * rows : (i + 1) * rows])
    bit = 2
    while bit < 2 * len(stay):
        for index in [i for i in sorted(held, reverse=True) if i & bit]:
            came = swap(held.pop(index), "tp", bit)
            held[index ^ bit] = add_rounded(held[index ^ bit], came)
        bit *= 2
    return held[0]


def add_rounded(first, second):
    return (first.astype(jnp.float32) + second.astype(jnp.float32)).astype(jnp.bfloat16)


def per_device(
    queries,
    key_rows,
    value_rows,
    lambdas,
    head_gain,
    out_weight,
    moe_input,
    moe_gain,
    routes,
    route_logits,
    expert_gate,
    expert_up,
    expert_down,
):
    ep, tp = lax.axis_size("ep"), lax.axis_size("tp")
    me, column = lax.axis_index("ep"), lax.axis_index("tp")
    far = ep // 2
    tokens, top_count = routes.shape
    cap = capacity(tokens, top_count, ep)

    hops = jnp.bitwise_xor(routes.T, me)
    ranks, outgoing = dispatch(moe_input, moe_gain, hops, cap, ep)
    ranks = window(ranks, expert_gate[0], expert_up[0], expert_down[0])
    quarter = ep // 4
    groups = [range(0, far), range(far, far + quarter), range(far + quarter, ep)]

    local_rows, local_heads = queries.shape[0], lambdas.shape[0]
    half = local_heads // 2
    mine = (me // far).astype(jnp.int32)

    def halves(array):
        width = array.shape[1] // 2
        first, second = array[:, :width], array[:, width:]
        keep = jnp.where(mine == 0, first, second)
        give = jnp.where(mine == 0, second, first)
        return keep, give

    parts = local_rows // tp
    ordered = jnp.concatenate(
        [
            lax.dynamic_slice_in_dim(queries, jnp.bitwise_xor(column, b) * parts, parts, 0)
            for b in range(tp)
        ],
        axis=0,
    )
    q_keep, q_give = halves(ordered)
    k_keep, k_give = halves(key_rows)
    v_keep, v_give = halves(value_rows)
    kept = jnp.concatenate([k_keep, v_keep], axis=1)
    given = jnp.concatenate([k_give, v_give, q_give], axis=1)
    came = swap(given, "ep", far)
    kv_width = kept.shape[1]
    came_kv, came_q = came[:, :kv_width], came[:, kv_width:]
    key_blocks = gather_all(kept, "ep", far) + gather_all(came_kv, "ep", far)

    arrived = {0: outgoing[0]}
    for group in (groups[1], groups[0], groups[2]):
        for k in group:
            if k:
                arrived[k] = swap(outgoing[k], "ep", k)

    sent_out = attention(mine, lambdas, head_gain, came_q, key_blocks, half)
    returned = swap(sent_out, "ep", far)
    kept_out = attention(mine, lambdas, head_gain, q_keep, key_blocks, half)
    both = jnp.concatenate([kept_out, returned], axis=1)
    moved = [both[b * parts : (b + 1) * parts] for b in range(tp)]
    moved = [swap(block, "tp", b) if b else block for b, block in enumerate(moved)]
    half_rows = out_weight.shape[0] // 2
    first_rows = gather_all(out_weight[:half_rows], "tp", tp)
    last_rows = gather_all(out_weight[half_rows:], "tp", tp)
    mixer_out = mixer(mine, moved, [w for pair in zip(first_rows, last_rows) for w in pair])

    replies = {}
    for group in groups:
        block = jnp.concatenate([arrived[k] for k in group], axis=0)
        blocks = gather_all(block, "tp", tp)
        partial = expert(blocks, expert_gate[0], expert_up[0], expert_down[0])
        summed = scatter_tp(partial[:-1], partial[-1])
        for index, k in enumerate(group):
            piece = summed[index * cap : (index + 1) * cap]
            replies[k] = swap(piece, "ep", k) if k else piece
    expert_out = combine(hops, ranks, route_logits.T, [replies[k] for k in range(ep)])
    return (mixer_out, expert_out)


def solution(mesh):
    placed = (
        P("ep", "tp"),
        P("ep", "tp"),
        P("ep", "tp"),
        P("tp"),
        P(),
        P("tp", None),
        P(("ep", "tp"), None),
        P(),
        P(("ep", "tp"), None),
        P(("ep", "tp"), None),
        P("ep", None, "tp"),
        P("ep", None, "tp"),
        P("ep", "tp", None),
    )
    return jax.shard_map(
        per_device,
        mesh=mesh,
        in_specs=placed,
        out_specs=(P(("ep", "tp"), None), P(("ep", "tp"), None)),
        check_vma=False,
    )
```

profile of v0, /device:TPU:0, one launch (start us, length us, event | category | flops | bytes accessed | tf_op | source)
XLA Modules:
  0.0 196.9 jit_solution(12067173291212502112)
XLA Ops:
  3.7 5.1 %collective-permute-start.37 = (bf16[40,2048]{1,0:T(8,128)(2,1)S(1)}, bf16[40,2048]{1,0:T(8,128)(2,1)}, u32[]{:S(2)}, u32[]{:S(2)}) collective-permute-start(bf16[40,2048]{1,0:T(8,128)(2,1)S(1)} %get-tuple-element.33), channel_id=1, source_target_pairs={{0,24},{4,28},{8,16},{12,20},{16,8},{20,12},{24,0},{28,4},{1,25},{... | collective-permute-start | bytes 491528 | tf_op jit(solution)/shard_map/ppermute | solution.py:27
  10.9 1.9 collective-permute-start.29
  12.8 1.7 collective-permute-start.17
  17.0 10.9 %collective-permute-start.18 = (bf16[40,2048]{1,0:T(8,128)(2,1)S(1)}, bf16[40,2048]{1,0:T(8,128)(2,1)S(1)}, u32[]{:S(2)}, u32[]{:S(2)}) collective-permute-start(bf16[40,2048]{1,0:T(8,128)(2,1)S(1)} %get-tuple-element.23), channel_id=1, source_target_pairs={{0,8},{4,12},{8,0},{12,4},{16,24},{20,28},{24,16},{28,20},{1,9},{5... | collective-permute-start | bytes 491528 | tf_op jit(solution)/shard_map/ppermute | solution.py:27
  28.8 5.6 %collective-permute-done.28 = bf16[40,2048]{1,0:T(8,128)(2,1)} collective-permute-done((bf16[40,2048]{1,0:T(8,128)(2,1)S(1)}, bf16[40,2048]{1,0:T(8,128)(2,1)}, u32[]{:S(2)}, u32[]{:S(2)}) %collective-permute-start.28) | collective-permute-done | bytes 163872 | tf_op jit(solution)/shard_map/ppermute | solution.py:27
  36.0 3.6 %collective-permute-start.3 = (bf16[512,384]{1,0:T(8,128)(2,1)S(1)}, bf16[512,384]{1,0:T(8,128)(2,1)S(1)}, u32[]{:S(2)}, u32[]{:S(2)}) collective-permute-start(bf16[512,384]{1,0:T(8,128)(2,1)S(1)} %pad_maximum_fusion), channel_id=1, source_target_pairs={{0,16},{4,20},{8,24},{12,28},{16,0},{20,4},{24,8},{28,12},{1,17},{... | collective-permute-start | bytes 1179656 | tf_op jit(solution)/shard_map/ppermute | solution.py:27
  40.6 1.6 collective-permute-start.40
  43.8 5.3 %collective-permute-done.40.refs_2_ = bf16[80,2048]{1,0:T(8,128)(2,1)S(1)} collective-permute-done((bf16[80,2048]{1,0:T(8,128)(2,1)S(1)}, bf16[80,2048]{1,0:T(8,128)(2,1)S(1)}, u32[]{:S(2)}, u32[]{:S(2)}) %collective-permute-start.40) | collective-permute-done | bytes 327712 | tf_op jit(solution)/shard_map/ppermute | solution.py:27
  49.2 5.8 %collective-permute-done.3 = bf16[512,384]{1,0:T(8,128)(2,1)S(1)} collective-permute-done((bf16[512,384]{1,0:T(8,128)(2,1)S(1)}, bf16[512,384]{1,0:T(8,128)(2,1)S(1)}, u32[]{:S(2)}, u32[]{:S(2)}) %collective-permute-start.3) | collective-permute-done | bytes 393248 | tf_op jit(solution)/shard_map/ppermute | solution.py:27
  55.1 1.6 collective-permute-start.21
  56.9 2.0 %copy-done.1 = bf16[1,2048,896]{2,1,0:T(8,128)(2,1)S(1)} copy-done((bf16[1,2048,896]{2,1,0:T(8,128)(2,1)S(1)}, bf16[1,2048,896]{2,1,0:T(8,128)(2,1)}, u32[]{:S(2)}) %copy-start.1) | copy-done | bytes 3670040
  59.0 2.0 %copy-done.3 = bf16[1,896,2048]{2,1,0:T(8,128)(2,1)S(1)} copy-done((bf16[1,896,2048]{2,1,0:T(8,128)(2,1)S(1)}, bf16[1,896,2048]{2,1,0:T(8,128)(2,1)}, u32[]{:S(2)}) %copy-start.3) | copy-done | bytes 3670040
  61.0 5.8 %shard_map.144 = (bf16[80,2048]{1,0:T(8,128)(2,1)S(1)}, bf16[80,2048]{1,0:T(8,128)(2,1)S(1)}, bf16[160,2048]{1,0:T(8,128)(2,1)S(1)}) custom-call(bf16[80,2048]{1,0:T(8,128)(2,1)S(1)} %constant_dynamic-update-slice_fusion.6.refs_0_, bf16[80,2048]{1,0:T(8,128)(2,1)S(1)} %collective-permute-done.39.refs_1_, ...), custom_call_target="tpu_custom_call" | custom-call | flops 3523215360 | bytes 13631488 | tf_op jit(solution)/shard_map/pallas_call | solution.py:177
  71.0 6.0 %shard_map.143 = (bf16[80,2048]{1,0:T(8,128)(2,1)S(1)}, bf16[80,2048]{1,0:T(8,128)(2,1)S(1)}, bf16[160,2048]{1,0:T(8,128)(2,1)S(1)}) custom-call(bf16[80,2048]{1,0:T(8,128)(2,1)S(1)} %constant_dynamic-update-slice_fusion.4.refs_0_, bf16[80,2048]{1,0:T(8,128)(2,1)S(1)} %collective-permute-done.30.refs_1_, ...), custom_call_target="tpu_custom_call" | custom-call | flops 3523215360 | bytes 13631488 | tf_op jit(solution)/shard_map/pallas_call | solution.py:177
  77.5 4.2 %collective-permute-done.2.refs_3_ = bf16[512,256]{1,0:T(8,128)(2,1)S(1)} collective-permute-done((bf16[512,256]{1,0:T(8,128)(2,1)S(1)}, bf16[512,256]{1,0:T(8,128)(2,1)S(1)}, u32[]{:S(2)}, u32[]{:S(2)}) %collective-permute-start.2) | collective-permute-done | bytes 262176 | tf_op jit(solution)/shard_map/ppermute | solution.py:27
  81.7 5.6 %collective-permute-done.4.refs_5_ = bf16[512,256]{1,0:T(8,128)(2,1)S(1)} collective-permute-done((bf16[512,256]{1,0:T(8,128)(2,1)S(1)}, bf16[512,256]{1,0:T(8,128)(2,1)S(1)}, u32[]{:S(2)}, u32[]{:S(2)}) %collective-permute-start.4) | collective-permute-done | bytes 262176 | tf_op jit(solution)/shard_map/ppermute | solution.py:27
  87.8 4.4 %collective-permute-done.6.refs_7_ = bf16[512,256]{1,0:T(8,128)(2,1)S(1)} collective-permute-done((bf16[512,256]{1,0:T(8,128)(2,1)S(1)}, bf16[512,256]{1,0:T(8,128)(2,1)S(1)}, u32[]{:S(2)}, u32[]{:S(2)}) %collective-permute-start.6) | collective-permute-done | bytes 262176 | tf_op jit(solution)/shard_map/ppermute | solution.py:27
  92.3 7.2 %shard_map.141 = bf16[512,128]{1,0:T(8,128)(2,1)S(1)} custom-call(s32[1]{0:T(128)} %bitcast.mine_ref, f32[2]{0:T(128)S(1)} %copy-done.8, f32[1,128]{1,0:T(1,128)S(1)} %bitcast.23, bf16[512,128]{1,0:T(8,128)(2,1)S(1)} %slice.115.q_ref, bf16[512,256]{1,0:T(8,128)(2,1)S(1)} %pad_maximum_fusion.2.refs_0_, bf16[512,256]{1,0:T(8,128)(2,1)S(1)} %collective-permute-done.refs_1_, ...), custom_call_target="tpu_custom_call" | custom-call | flops 3221225472 | bytes 2097152 | tf_op jit(solution)/shard_map/pallas_call | solution.py:267
  99.5 2.0 %collective-permute-start.7 = (bf16[512,128]{1,0:T(8,128)(2,1)S(1)}, bf16[512,128]{1,0:T(8,128)(2,1)S(1)}, u32[]{:S(2)}, u32[]{:S(2)}) collective-permute-start(bf16[512,128]{1,0:T(8,128)(2,1)S(1)} %shard_map.141), channel_id=1, source_target_pairs={{0,16},{4,20},{8,24},{12,28},{16,0},{20,4},{24,8},{28,12},{1,17},{... | collective-permute-start | bytes 393224 | tf_op jit(solution)/shard_map/ppermute | solution.py:27
  101.5 7.4 %shard_map.140 = bf16[512,128]{1,0:T(8,128)(2,1)S(1)} custom-call(s32[1]{0:T(128)} %bitcast.mine_ref, f32[2]{0:T(128)S(1)} %copy-done.8, f32[1,128]{1,0:T(1,128)S(1)} %bitcast.24, bf16[512,128]{1,0:T(8,128)(2,1)S(1)} %get-tuple-element.57.q_ref, bf16[512,256]{1,0:T(8,128)(2,1)S(1)} %pad_maximum_fusion.2.refs_0_, ...), custom_call_target="tpu_custom_call" | custom-call | flops 3221225472 | bytes 2097152 | tf_op jit(solution)/shard_map/pallas_call | solution.py:267
  111.6 9.5 %shard_map.142 = (bf16[160,2048]{1,0:T(8,128)(2,1)S(1)}, bf16[160,2048]{1,0:T(8,128)(2,1)S(1)}, bf16[320,2048]{1,0:T(8,128)(2,1)S(1)}) custom-call(bf16[160,2048]{1,0:T(8,128)(2,1)S(1)} %constant_dynamic-update-slice_fusion.refs_0_, bf16[160,2048]{1,0:T(8,128)(2,1)S(1)} %collective-permute-done.20.refs_1_, ...), custom_call_target="tpu_custom_call" | custom-call | flops 7046430720 | bytes 16252928 | tf_op jit(solution)/shard_map/pallas_call | solution.py:177
  121.3 9.3 %collective-permute-done.43 = bf16[80,2048]{1,0:T(8,128)(2,1)S(1)} collective-permute-done((bf16[80,2048]{1,0:T(8,128)(2,1)S(1)}, bf16[80,2048]{1,0:T(8,128)(2,1)S(1)}, u32[]{:S(2)}, u32[]{:S(2)}) %collective-permute-start.43) | collective-permute-done | bytes 327712 | tf_op jit(solution)/shard_map/ppermute | solution.py:27
  131.8 8.0 %collective-permute-done.34 = bf16[80,2048]{1,0:T(8,128)(2,1)S(1)} collective-permute-done((bf16[80,2048]{1,0:T(8,128)(2,1)S(1)}, bf16[80,2048]{1,0:T(8,128)(2,1)S(1)}, u32[]{:S(2)}, u32[]{:S(2)}) %collective-permute-start.34) | collective-permute-done | bytes 327712 | tf_op jit(solution)/shard_map/ppermute | solution.py:27
  140.8 16.6 %collective-permute-done.24 = bf16[160,2048]{1,0:T(8,128)(2,1)S(1)} collective-permute-done((bf16[160,2048]{1,0:T(8,128)(2,1)S(1)}, bf16[160,2048]{1,0:T(8,128)(2,1)S(1)}, u32[]{:S(2)}, u32[]{:S(2)}) %collective-permute-start.24) | collective-permute-done | bytes 655392 | tf_op jit(solution)/shard_map/ppermute | solution.py:27
  159.9 2.3 %collective-permute-start.44 = (bf16[40,2048]{1,0:T(8,128)(2,1)S(1)}, bf16[40,2048]{1,0:T(8,128)(2,1)S(1)}, u32[]{:S(2)}, u32[]{:S(2)}) collective-permute-start(bf16[40,2048]{1,0:T(8,128)(2,1)S(1)} %get-tuple-element.45), channel_id=1, source_target_pairs={{0,24},{4,28},{8,16},{12,20},{16,8},{20,12},{24,0},{28,4},{1,25},{... | collective-permute-start | bytes 491528 | tf_op jit(solution)/shard_map/ppermute | solution.py:27
  162.2 2.3 %collective-permute-start.45 = (bf16[40,2048]{1,0:T(8,128)(2,1)S(1)}, bf16[40,2048]{1,0:T(8,128)(2,1)S(1)}, u32[]{:S(2)}, u32[]{:S(2)}) collective-permute-start(bf16[40,2048]{1,0:T(8,128)(2,1)S(1)} %get-tuple-element.44), channel_id=1, source_target_pairs={{0,28},{4,24},{8,20},{12,16},{16,12},{20,8},{24,4},{28,0},{1,29},{... | collective-permute-start | bytes 491528 | tf_op jit(solution)/shard_map/ppermute | solution.py:27
  164.7 3.0 %collective-permute-start.36 = (bf16[40,2048]{1,0:T(8,128)(2,1)S(1)}, bf16[40,2048]{1,0:T(8,128)(2,1)S(1)}, u32[]{:S(2)}, u32[]{:S(2)}) collective-permute-start(bf16[40,2048]{1,0:T(8,128)(2,1)S(1)} %get-tuple-element.46), channel_id=1, source_target_pairs={{0,20},{4,16},{8,28},{12,24},{16,4},{20,0},{24,12},{28,8},{1,21},{... | collective-permute-start | bytes 491528 | tf_op jit(solution)/shard_map/ppermute | solution.py:27
  169.1 12.0 %collective-permute-start.26 = (bf16[40,2048]{1,0:T(8,128)(2,1)S(1)}, bf16[40,2048]{1,0:T(8,128)(2,1)S(1)}, u32[]{:S(2)}, u32[]{:S(2)}) collective-permute-start(bf16[40,2048]{1,0:T(8,128)(2,1)S(1)} %get-tuple-element.41), channel_id=1, source_target_pairs={{0,8},{4,12},{8,0},{12,4},{16,24},{20,28},{24,16},{28,20},{1,9},{5... | collective-permute-start | bytes 491528 | tf_op jit(solution)/shard_map/ppermute | solution.py:27
  181.1 4.4 %collective-permute-start.27 = (bf16[40,2048]{1,0:T(8,128)(2,1)S(1)}, bf16[40,2048]{1,0:T(8,128)(2,1)S(1)}, u32[]{:S(2)}, u32[]{:S(2)}) collective-permute-start(bf16[40,2048]{1,0:T(8,128)(2,1)S(1)} %get-tuple-element.40), channel_id=1, source_target_pairs={{0,12},{4,8},{8,4},{12,0},{16,28},{20,24},{24,20},{28,16},{1,13},{... | collective-permute-start | bytes 491528 | tf_op jit(solution)/shard_map/ppermute | solution.py:27
  187.6 3.2 %collective-permute-done.36.refs_5_ = bf16[40,2048]{1,0:T(8,128)(2,1)S(1)} collective-permute-done((bf16[40,2048]{1,0:T(8,128)(2,1)S(1)}, bf16[40,2048]{1,0:T(8,128)(2,1)S(1)}, u32[]{:S(2)}, u32[]{:S(2)}) %collective-permute-start.36) | collective-permute-done | bytes 163872 | tf_op jit(solution)/shard_map/ppermute | solution.py:27
  191.9 3.3 %collective-permute-done.27.refs_3_ = bf16[40,2048]{1,0:T(8,128)(2,1)S(1)} collective-permute-done((bf16[40,2048]{1,0:T(8,128)(2,1)S(1)}, bf16[40,2048]{1,0:T(8,128)(2,1)S(1)}, u32[]{:S(2)}, u32[]{:S(2)}) %collective-permute-start.27) | collective-permute-done | bytes 163872 | tf_op jit(solution)/shard_map/ppermute | solution.py:27
  195.3 1.6 combine.1
  (123 shorter events, 30.4 us)
Async XLA Ops:
  3.7 13.2 %collective-permute-start.37 = (bf16[40,2048]{1,0:T(8,128)(2,1)S(1)}, bf16[40,2048]{1,0:T(8,128)(2,1)}, u32[]{:S(2)}, u32[]{:S(2)}) collective-permute-start(bf16[40,2048]{1,0:T(8,128)(2,1)S(1)} %get-tuple-element.33), channel_id=1, source_target_pairs={{0,24},{4,28},{8,16},{12,20},{16,8},{20,12},{24,0},{28,4},{1,25},{... | collective-permute-start | bytes 491528 | tf_op jit(solution)/shard_map/ppermute | solution.py:27
  8.9 27.1 %collective-permute-start.38 = (bf16[40,2048]{1,0:T(8,128)(2,1)S(1)}, bf16[40,2048]{1,0:T(8,128)(2,1)}, u32[]{:S(2)}, u32[]{:S(2)}) collective-permute-start(bf16[40,2048]{1,0:T(8,128)(2,1)S(1)} %get-tuple-element.34), channel_id=1, source_target_pairs={{0,28},{4,24},{8,20},{12,16},{16,12},{20,8},{24,4},{28,0},{1,29},{... | collective-permute-start | bytes 491528 | tf_op jit(solution)/shard_map/ppermute | solution.py:27
  10.1 24.4 %collective-permute-start.28 = (bf16[40,2048]{1,0:T(8,128)(2,1)S(1)}, bf16[40,2048]{1,0:T(8,128)(2,1)}, u32[]{:S(2)}, u32[]{:S(2)}) collective-permute-start(bf16[40,2048]{1,0:T(8,128)(2,1)S(1)} %get-tuple-element.28), channel_id=1, source_target_pairs={{0,16},{4,20},{8,24},{12,28},{16,0},{20,4},{24,8},{28,12},{1,17},{... | collective-permute-start | bytes 491528 | tf_op jit(solution)/shard_map/ppermute | solution.py:27
  10.9 29.7 %collective-permute-start.29 = (bf16[40,2048]{1,0:T(8,128)(2,1)S(1)}, bf16[40,2048]{1,0:T(8,128)(2,1)}, u32[]{:S(2)}, u32[]{:S(2)}) collective-permute-start(bf16[40,2048]{1,0:T(8,128)(2,1)S(1)} %get-tuple-element.29), channel_id=1, source_target_pairs={{0,20},{4,16},{8,28},{12,24},{16,4},{20,0},{24,12},{28,8},{1,21},{... | collective-permute-start | bytes 491528 | tf_op jit(solution)/shard_map/ppermute | solution.py:27
  12.8 30.3 %collective-permute-start.17 = (bf16[40,2048]{1,0:T(8,128)(2,1)S(1)}, bf16[40,2048]{1,0:T(8,128)(2,1)S(1)}, u32[]{:S(2)}, u32[]{:S(2)}) collective-permute-start(bf16[40,2048]{1,0:T(8,128)(2,1)S(1)} %get-tuple-element.22), channel_id=1, source_target_pairs={{0,4},{4,0},{8,12},{12,8},{16,20},{20,16},{24,28},{28,24},{1,5},{5... | collective-permute-start | bytes 491528 | tf_op jit(solution)/shard_map/ppermute | solution.py:27
  17.0 26.2 %collective-permute-start.18 = (bf16[40,2048]{1,0:T(8,128)(2,1)S(1)}, bf16[40,2048]{1,0:T(8,128)(2,1)S(1)}, u32[]{:S(2)}, u32[]{:S(2)}) collective-permute-start(bf16[40,2048]{1,0:T(8,128)(2,1)S(1)} %get-tuple-element.23), channel_id=1, source_target_pairs={{0,8},{4,12},{8,0},{12,4},{16,24},{20,28},{24,16},{28,20},{1,9},{5... | collective-permute-start | bytes 491528 | tf_op jit(solution)/shard_map/ppermute | solution.py:27
  34.5 14.7 %collective-permute-start.19 = (bf16[40,2048]{1,0:T(8,128)(2,1)S(1)}, bf16[40,2048]{1,0:T(8,128)(2,1)S(1)}, u32[]{:S(2)}, u32[]{:S(2)}) collective-permute-start(bf16[40,2048]{1,0:T(8,128)(2,1)S(1)} %get-tuple-element.24), channel_id=1, source_target_pairs={{0,12},{4,8},{8,4},{12,0},{16,28},{20,24},{24,20},{28,16},{1,13},{... | collective-permute-start | bytes 491528 | tf_op jit(solution)/shard_map/ppermute | solution.py:27
  36.0 19.0 %collective-permute-start.3 = (bf16[512,384]{1,0:T(8,128)(2,1)S(1)}, bf16[512,384]{1,0:T(8,128)(2,1)S(1)}, u32[]{:S(2)}, u32[]{:S(2)}) collective-permute-start(bf16[512,384]{1,0:T(8,128)(2,1)S(1)} %pad_maximum_fusion), channel_id=1, source_target_pairs={{0,16},{4,20},{8,24},{12,28},{16,0},{20,4},{24,8},{28,12},{1,17},{... | collective-permute-start | bytes 1179656 | tf_op jit(solution)/shard_map/ppermute | solution.py:27
  43.2 13.4 %collective-permute-start.31 = (bf16[80,2048]{1,0:T(8,128)(2,1)S(1)}, bf16[80,2048]{1,0:T(8,128)(2,1)S(1)}, u32[]{:S(2)}, u32[]{:S(2)}) collective-permute-start(bf16[80,2048]{1,0:T(8,128)(2,1)S(1)} %constant_dynamic-update-slice_fusion.4.refs_0_), channel_id=1, source_target_pairs={{0,2},{1,3},{2,0},{3,1},{4,6},{5,7},{6,4},{7,5},{8,10},{9,11},{10,... | collective-permute-start | bytes 983048 | tf_op jit(solution)/shard_map/ppermute | solution.py:27
  49.1 17.7 %collective-permute-start.1 = (bf16[512,256]{1,0:T(8,128)(2,1)S(1)}, bf16[512,256]{1,0:T(8,128)(2,1)S(1)}, u32[]{:S(2)}, u32[]{:S(2)}) collective-permute-start(bf16[512,256]{1,0:T(8,128)(2,1)S(1)} %pad_maximum_fusion.2.refs_0_), channel_id=1, source_target_pairs={{0,8},{4,12},{8,0},{12,4},{16,24},{20,28},{24,16},{28,20},{1,9},{5... | collective-permute-start | bytes 786440 | tf_op jit(solution)/shard_map/ppermute | solution.py:27
  55.1 32.3 %collective-permute-start.21 = (bf16[160,2048]{1,0:T(8,128)(2,1)S(1)}, bf16[160,2048]{1,0:T(8,128)(2,1)S(1)}, u32[]{:S(2)}, u32[]{:S(2)}) collective-permute-start(bf16[160,2048]{1,0:T(8,128)(2,1)S(1)} %constant_dynamic-update-slice_fusion.refs_0_), channel_id=1, source_target_pairs={{0,2},{1,3},{2,0},{3,1},{4,6},{5,7},{6,4},{7,5},{8,10},{9,11},{10,... | collective-permute-start | bytes 1966088 | tf_op jit(solution)/shard_map/ppermute | solution.py:27
  67.5 14.2 %collective-permute-start.2 = (bf16[512,256]{1,0:T(8,128)(2,1)S(1)}, bf16[512,256]{1,0:T(8,128)(2,1)S(1)}, u32[]{:S(2)}, u32[]{:S(2)}) collective-permute-start(bf16[512,256]{1,0:T(8,128)(2,1)S(1)} %collective-permute-done.1.refs_2_), channel_id=1, source_target_pairs={{0,4},{4,0},{8,12},{12,8},{16,20},{20,16},{24,28},{28,24},{1,5},{5... | collective-permute-start | bytes 786440 | tf_op jit(solution)/shard_map/ppermute | solution.py:27
  68.9 18.4 %collective-permute-start.4 = (bf16[512,256]{1,0:T(8,128)(2,1)S(1)}, bf16[512,256]{1,0:T(8,128)(2,1)S(1)}, u32[]{:S(2)}, u32[]{:S(2)}) collective-permute-start(bf16[512,256]{1,0:T(8,128)(2,1)S(1)} %slice.114.refs_4_), channel_id=1, source_target_pairs={{0,4},{4,0},{8,12},{12,8},{16,20},{20,16},{24,28},{28,24},{1,5},{5... | collective-permute-start | bytes 786440 | tf_op jit(solution)/shard_map/ppermute | solution.py:27
  69.5 22.8 %collective-permute-start.6 = (bf16[512,256]{1,0:T(8,128)(2,1)S(1)}, bf16[512,256]{1,0:T(8,128)(2,1)S(1)}, u32[]{:S(2)}, u32[]{:S(2)}) collective-permute-start(bf16[512,256]{1,0:T(8,128)(2,1)S(1)} %collective-permute-done.5.refs_6_), channel_id=1, source_target_pairs={{0,4},{4,0},{8,12},{12,8},{16,20},{20,16},{24,28},{28,24},{1,5},{5... | collective-permute-start | bytes 786440 | tf_op jit(solution)/shard_map/ppermute | solution.py:27
  77.0 54.2 %collective-permute-start.13 = (bf16[128,2048]{1,0:T(8,128)(2,1)S(1)}, bf16[128,2048]{1,0:T(8,128)(2,1)S(1)}, u32[]{:S(2)}, u32[]{:S(2)}) collective-permute-start(bf16[128,2048]{1,0:T(8,128)(2,1)S(1)} %get-tuple-element.39.refs_4_), channel_id=1, source_target_pairs={{0,2},{1,3},{2,0},{3,1},{4,6},{5,7},{6,4},{7,5},{8,10},{9,11},{10,... | collective-permute-start | bytes 1572872 | tf_op jit(solution)/shard_map/ppermute | solution.py:27
  81.7 28.1 %collective-permute-start.20 = (bf16[160,2048]{1,0:T(8,128)(2,1)S(1)}, bf16[160,2048]{1,0:T(8,128)(2,1)S(1)}, u32[]{:S(2)}, u32[]{:S(2)}) collective-permute-start(bf16[160,2048]{1,0:T(8,128)(2,1)S(1)} %constant_dynamic-update-slice_fusion.refs_0_), channel_id=1, source_target_pairs={{0,1},{1,0},{2,3},{3,2},{4,5},{5,4},{6,7},{7,6},{8,9},{9,8},{10,11... | collective-permute-start | bytes 1966088 | tf_op jit(solution)/shard_map/ppermute | solution.py:27
  87.3 21.8 %collective-permute-start.42 = (bf16[160,2048]{1,0:T(8,128)(2,1)S(1)}, bf16[160,2048]{1,0:T(8,128)(2,1)S(1)}, u32[]{:S(2)}, u32[]{:S(2)}) collective-permute-start(bf16[160,2048]{1,0:T(8,128)(2,1)S(1)} %get-tuple-element.36), channel_id=1, source_target_pairs={{0,1},{1,0},{2,3},{3,2},{4,5},{5,4},{6,7},{7,6},{8,9},{9,8},{10,11... | collective-permute-start | bytes 1966088 | tf_op jit(solution)/shard_map/ppermute | solution.py:27
  87.3 22.8 %collective-permute-start.22 = (bf16[160,2048]{1,0:T(8,128)(2,1)S(1)}, bf16[160,2048]{1,0:T(8,128)(2,1)S(1)}, u32[]{:S(2)}, u32[]{:S(2)}) collective-permute-start(bf16[160,2048]{1,0:T(8,128)(2,1)S(1)} %collective-permute-done.21.refs_2_), channel_id=1, source_target_pairs={{0,1},{1,0},{2,3},{3,2},{4,5},{5,4},{6,7},{7,6},{8,9},{9,8},{10,11... | collective-permute-start | bytes 1966088 | tf_op jit(solution)/shard_map/ppermute | solution.py:27
  109.0 48.7 %collective-permute-start.11 = (bf16[128,2048]{1,0:T(8,128)(2,1)S(1)}, bf16[128,2048]{1,0:T(8,128)(2,1)S(1)}, u32[]{:S(2)}, u32[]{:S(2)}) collective-permute-start(bf16[128,2048]{1,0:T(8,128)(2,1)S(1)} %get-tuple-element.39.refs_4_), channel_id=1, source_target_pairs={{0,1},{1,0},{2,3},{3,2},{4,5},{5,4},{6,7},{7,6},{8,9},{9,8},{10,11... | collective-permute-start | bytes 1572872 | tf_op jit(solution)/shard_map/ppermute | solution.py:27
  109.1 22.1 %collective-permute-start.14 = (bf16[128,2048]{1,0:T(8,128)(2,1)S(1)}, bf16[128,2048]{1,0:T(8,128)(2,1)S(1)}, u32[]{:S(2)}, u32[]{:S(2)}) collective-permute-start(bf16[128,2048]{1,0:T(8,128)(2,1)S(1)} %get-tuple-element.38.refs_5_), channel_id=1, source_target_pairs={{0,2},{1,3},{2,0},{3,1},{4,6},{5,7},{6,4},{7,5},{8,10},{9,11},{10,... | collective-permute-start | bytes 1572872 | tf_op jit(solution)/shard_map/ppermute | solution.py:27
  110.1 20.4 %collective-permute-start.43 = (bf16[80,2048]{1,0:T(8,128)(2,1)S(1)}, bf16[80,2048]{1,0:T(8,128)(2,1)S(1)}, u32[]{:S(2)}, u32[]{:S(2)}) collective-permute-start(bf16[80,2048]{1,0:T(8,128)(2,1)S(1)} %add_convert_fusion.4), channel_id=1, source_target_pairs={{0,2},{1,3},{2,0},{3,1},{4,6},{5,7},{6,4},{7,5},{8,10},{9,11},{10,... | collective-permute-start | bytes 983048 | tf_op jit(solution)/shard_map/ppermute | solution.py:27
  121.1 18.8 %collective-permute-start.23 = (bf16[320,2048]{1,0:T(8,128)(2,1)S(1)}, bf16[320,2048]{1,0:T(8,128)(2,1)S(1)}, u32[]{:S(2)}, u32[]{:S(2)}) collective-permute-start(bf16[320,2048]{1,0:T(8,128)(2,1)S(1)} %get-tuple-element.26), channel_id=1, source_target_pairs={{0,1},{1,0},{2,3},{3,2},{4,5},{5,4},{6,7},{7,6},{8,9},{9,8},{10,11... | collective-permute-start | bytes 3932168 | tf_op jit(solution)/shard_map/ppermute | solution.py:27
  131.2 27.2 %collective-permute-start.12 = (bf16[128,2048]{1,0:T(8,128)(2,1)S(1)}, bf16[128,2048]{1,0:T(8,128)(2,1)S(1)}, u32[]{:S(2)}, u32[]{:S(2)}) collective-permute-start(bf16[128,2048]{1,0:T(8,128)(2,1)S(1)} %get-tuple-element.38.refs_5_), channel_id=1, source_target_pairs={{0,1},{1,0},{2,3},{3,2},{4,5},{5,4},{6,7},{7,6},{8,9},{9,8},{10,11... | collective-permute-start | bytes 1572872 | tf_op jit(solution)/shard_map/ppermute | solution.py:27
  131.3 28.6 %collective-permute-start.15 = (bf16[128,2048]{1,0:T(8,128)(2,1)S(1)}, bf16[128,2048]{1,0:T(8,128)(2,1)S(1)}, u32[]{:S(2)}, u32[]{:S(2)}) collective-permute-start(bf16[128,2048]{1,0:T(8,128)(2,1)S(1)} %collective-permute-done.13.refs_8_), channel_id=1, source_target_pairs={{0,1},{1,0},{2,3},{3,2},{4,5},{5,4},{6,7},{7,6},{8,9},{9,8},{10,11... | collective-permute-start | bytes 1572872 | tf_op jit(solution)/shard_map/ppermute | solution.py:27
  139.8 22.4 %collective-permute-start.16 = (bf16[128,2048]{1,0:T(8,128)(2,1)S(1)}, bf16[128,2048]{1,0:T(8,128)(2,1)S(1)}, u32[]{:S(2)}, u32[]{:S(2)}) collective-permute-start(bf16[128,2048]{1,0:T(8,128)(2,1)S(1)} %collective-permute-done.14.refs_9_), channel_id=1, source_target_pairs={{0,1},{1,0},{2,3},{3,2},{4,5},{5,4},{6,7},{7,6},{8,9},{9,8},{10,11... | collective-permute-start | bytes 1572872 | tf_op jit(solution)/shard_map/ppermute | solution.py:27
  140.1 17.2 %collective-permute-start.24 = (bf16[160,2048]{1,0:T(8,128)(2,1)S(1)}, bf16[160,2048]{1,0:T(8,128)(2,1)S(1)}, u32[]{:S(2)}, u32[]{:S(2)}) collective-permute-start(bf16[160,2048]{1,0:T(8,128)(2,1)S(1)} %add_convert_fusion.1), channel_id=1, source_target_pairs={{0,2},{1,3},{2,0},{3,1},{4,6},{5,7},{6,4},{7,5},{8,10},{9,11},{10,... | collective-permute-start | bytes 1966088 | tf_op jit(solution)/shard_map/ppermute | solution.py:27
  162.2 18.8 %collective-permute-start.45 = (bf16[40,2048]{1,0:T(8,128)(2,1)S(1)}, bf16[40,2048]{1,0:T(8,128)(2,1)S(1)}, u32[]{:S(2)}, u32[]{:S(2)}) collective-permute-start(bf16[40,2048]{1,0:T(8,128)(2,1)S(1)} %get-tuple-element.44), channel_id=1, source_target_pairs={{0,28},{4,24},{8,20},{12,16},{16,12},{20,8},{24,4},{28,0},{1,29},{... | collective-permute-start | bytes 491528 | tf_op jit(solution)/shard_map/ppermute | solution.py:27
  164.6 23.0 %collective-permute-start.35 = (bf16[40,2048]{1,0:T(8,128)(2,1)S(1)}, bf16[40,2048]{1,0:T(8,128)(2,1)S(1)}, u32[]{:S(2)}, u32[]{:S(2)}) collective-permute-start(bf16[40,2048]{1,0:T(8,128)(2,1)S(1)} %get-tuple-element.47), channel_id=1, source_target_pairs={{0,16},{4,20},{8,24},{12,28},{16,0},{20,4},{24,8},{28,12},{1,17},{... | collective-permute-start | bytes 491528 | tf_op jit(solution)/shard_map/ppermute | solution.py:27
  164.7 26.1 %collective-permute-start.36 = (bf16[40,2048]{1,0:T(8,128)(2,1)S(1)}, bf16[40,2048]{1,0:T(8,128)(2,1)S(1)}, u32[]{:S(2)}, u32[]{:S(2)}) collective-permute-start(bf16[40,2048]{1,0:T(8,128)(2,1)S(1)} %get-tuple-element.46), channel_id=1, source_target_pairs={{0,20},{4,16},{8,28},{12,24},{16,4},{20,0},{24,12},{28,8},{1,21},{... | collective-permute-start | bytes 491528 | tf_op jit(solution)/shard_map/ppermute | solution.py:27
  167.7 23.1 %collective-permute-start.25 = (bf16[40,2048]{1,0:T(8,128)(2,1)S(1)}, bf16[40,2048]{1,0:T(8,128)(2,1)S(1)}, u32[]{:S(2)}, u32[]{:S(2)}) collective-permute-start(bf16[40,2048]{1,0:T(8,128)(2,1)S(1)} %get-tuple-element.42), channel_id=1, source_target_pairs={{0,4},{4,0},{8,12},{12,8},{16,20},{20,16},{24,28},{28,24},{1,5},{5... | collective-permute-start | bytes 491528 | tf_op jit(solution)/shard_map/ppermute | solution.py:27
  169.1 22.9 %collective-permute-start.26 = (bf16[40,2048]{1,0:T(8,128)(2,1)S(1)}, bf16[40,2048]{1,0:T(8,128)(2,1)S(1)}, u32[]{:S(2)}, u32[]{:S(2)}) collective-permute-start(bf16[40,2048]{1,0:T(8,128)(2,1)S(1)} %get-tuple-element.41), channel_id=1, source_target_pairs={{0,8},{4,12},{8,0},{12,4},{16,24},{20,28},{24,16},{28,20},{1,9},{5... | collective-permute-start | bytes 491528 | tf_op jit(solution)/shard_map/ppermute | solution.py:27
  181.1 14.2 %collective-permute-start.27 = (bf16[40,2048]{1,0:T(8,128)(2,1)S(1)}, bf16[40,2048]{1,0:T(8,128)(2,1)S(1)}, u32[]{:S(2)}, u32[]{:S(2)}) collective-permute-start(bf16[40,2048]{1,0:T(8,128)(2,1)S(1)} %get-tuple-element.40), channel_id=1, source_target_pairs={{0,12},{4,8},{8,4},{12,0},{16,28},{20,24},{24,20},{28,16},{1,13},{... | collective-permute-start | bytes 491528 | tf_op jit(solution)/shard_map/ppermute | solution.py:27
  (27 other events, 279.4 us)
where the time goes:
time: 197 us
  waiting for transfers between devices  73.1 us (37%)
  starting transfers between devices  69.2 us (35%)
  Pallas kernels  39.7 us (20%)
  local copies, waits for them, and re-layouts  11.9 us (6%)
    ppermute x46, waiting for transfers between devices, swap(): return lax.ppermute(array, axis, [(i, i ^ mask) for i in range(size)])  73.1 us
    ppermute x46, starting transfers between devices, swap(): return lax.ppermute(array, axis, [(i, i ^ mask) for i in range(size)])  69.2 us
    pallas_call x3, Pallas kernels, expert(): pl.pallas_call(functools.partial(expert_kernel, count), out_shape=shapes,...  21.2 us
    pallas_call x2, Pallas kernels, attention(): pl.pallas_call(functools.partial(attention_kernel, heads, head_size, valu...  14.7 us
    unnamed x31, local copies, waits for them, and re-layouts  8.64 us
  transfers between devices with their start and end apart: 46, of which 13 were waited for; matrix products, arithmetic and copies ran while one was open for 3% of the time, Pallas kernels for 19%

commit v1 on v0

--- a/solution.py
+++ b/solution.py
@@ -10,9 +10,9 @@
 
 epsilon = 1e-06
 init_lambda = 0.2
-small_vmem = 12 * 1024 * 1024
-expert_vmem = 24 * 1024 * 1024
-attention_vmem = 32 * 1024 * 1024
+small_vmem = 6 * 1024 * 1024
+expert_vmem = 10 * 1024 * 1024
+attention_margin = 3 * 1024 * 1024
 
 
 whole_vmem = pl.BlockSpec(memory_space=pltpu.VMEM)
@@ -27,13 +27,14 @@
     return lax.ppermute(array, axis, [(i, i ^ mask) for i in range(size)])
 
 
-def dispatch_kernel(cap, x_ref, gain_ref, hops_ref, ranks_ref, *blocks):
+def dispatch_kernel(cap, place_ref, x_ref, gain_ref, routes_ref, hops_ref, ranks_ref, *blocks):
     tokens, _ = x_ref.shape
     rows = x_ref[...].astype(jnp.float32)
     mean_square = jnp.mean(rows * rows, axis=-1, keepdims=True)
     normed = (rows * lax.rsqrt(mean_square + epsilon) * gain_ref[...]).astype(jnp.bfloat16)
     count = len(blocks)
-    top = hops_ref.shape[0]
+    top = routes_ref.shape[0]
+    hops_ref[...] = routes_ref[...] ^ place_ref[0]
     earlier = lax.broadcasted_iota(jnp.int32, (tokens, tokens), 0)
     later = lax.broadcasted_iota(jnp.int32, (tokens, tokens), 1)
     before = (earlier < later).astype(jnp.float32).astype(jnp.bfloat16)
@@ -61,20 +62,53 @@
         block[...] = rows[k * cap : (k + 1) * cap].astype(jnp.bfloat16)
 
 
-def dispatch(moe_input, moe_gain, hops, cap, count):
+def dispatch(place, moe_input, moe_gain, routes, cap, count):
     tokens, width = moe_input.shape
-    shapes = [jax.ShapeDtypeStruct(hops.shape, jnp.int32)]
+    shapes = [jax.ShapeDtypeStruct(routes.shape, jnp.int32)] * 2
     shapes += [jax.ShapeDtypeStruct((cap, width), jnp.bfloat16)] * count
     out = pl.pallas_call(
         functools.partial(dispatch_kernel, cap),
         out_shape=shapes,
-        in_specs=[whole_vmem] * 3,
+        in_specs=[pl.BlockSpec(memory_space=pltpu.SMEM)] + [whole_vmem] * 3,
         out_specs=[whole_vmem] * len(shapes),
         cost_estimate=pl.CostEstimate(flops=2 * cap * count * tokens * width, bytes_accessed=4 * tokens * width, transcendentals=0),
         compiler_params=pltpu.CompilerParams(vmem_limit_bytes=small_vmem),
         name="dispatch",
-    )(moe_input, moe_gain.reshape(1, -1), hops)
-    return out[0], list(out[1:])
+    )(place, moe_input, moe_gain.reshape(1, -1), routes)
+    return out[0], out[1], list(out[2:])
+
+
+def pack_kernel(count, place_ref, q_ref, k_ref, v_ref, kept_ref, given_ref, q_keep_ref):
+    first = place_ref[2] == 0
+    parts = q_ref.shape[0] // count
+    k_half, v_half = k_ref.shape[1] // 2, v_ref.shape[1] // 2
+
+    def halves(array):
+        width = array.shape[1] // 2
+        low, high = array[:, :width], array[:, width:]
+        return jnp.where(first, low, high), jnp.where(first, high, low)
+
+    kept_ref[:, :k_half], given_ref[:, :k_half] = halves(k_ref[...])
+    kept_ref[:, k_half:], given_ref[:, k_half : k_half + v_half] = halves(v_ref[...])
+    for b in range(count):
+        source = pl.ds(pl.multiple_of((place_ref[1] ^ b) * parts, parts), parts)
+        at = slice(b * parts, (b + 1) * parts)
+        q_keep_ref[at, :], given_ref[at, k_half + v_half :] = halves(q_ref[source, :])
+
+
+def pack(place, queries, keys, values, count):
+    rows = queries.shape[0]
+    q_half, k_half, v_half = queries.shape[1] // 2, keys.shape[1] // 2, values.shape[1] // 2
+    widths = (k_half + v_half, k_half + v_half + q_half, q_half)
+    return pl.pallas_call(
+        functools.partial(pack_kernel, count),
+        out_shape=[jax.ShapeDtypeStruct((rows, width), jnp.bfloat16) for width in widths],
+        in_specs=[pl.BlockSpec(memory_space=pltpu.SMEM)] + [whole_vmem] * 3,
+        out_specs=[whole_vmem] * 3,
+        compiler_params=pltpu.CompilerParams(vmem_limit_bytes=small_vmem),
+        cost_estimate=pl.CostEstimate(flops=rows, bytes_accessed=8 * rows * widths[1], transcendentals=0),
+        name="pack",
+    )(place, queries, keys, values)
 
 
 def window_kernel(ranks_ref, gate_ref, up_ref, down_ref, out_ref):
@@ -140,7 +174,7 @@
     gate_ref, up_ref, down_ref = refs[count : count + 3]
     outputs = refs[count + 3 : -1]
     hidden_ref = refs[-1]
-    _, width = inputs[0].shape
+    rows, width = inputs[0].shape
     tile, wide = 128, min(512, width)
     order = list(range(0, count, 2)) + list(range(1, count, 2))
 
@@ -163,8 +197,9 @@
             first += ref.shape[0]
         return carry
 
-    lax.fori_loop(0, gate_ref.shape[1] // tile, hidden_step, 0)
-    lax.fori_loop(0, width // wide, down_step, 0)
+    short = count * rows <= 512
+    lax.fori_loop(0, gate_ref.shape[1] // tile, hidden_step, 0, unroll=short)
+    lax.fori_loop(0, width // wide, down_step, 0, unroll=short)
 
 
 def expert(blocks, gate, up, down):
@@ -189,7 +224,7 @@
     )(*blocks, gate, up, down)
 
 
-def attention_kernel(heads, head_size, value_size, rows, count, mine_ref, lam_ref, gain_ref, q_ref, *refs):
+def attention_kernel(heads, head_size, value_size, rows, count, place_ref, lam_ref, gain_ref, q_ref, *refs):
     blocks, out_ref = refs[:count], refs[count]
     value_ref, score_a, score_b, peak_a, peak_b = refs[count + 1 :]
     tiles = q_ref.shape[0] // rows
@@ -199,7 +234,7 @@
     lanes = lax.broadcasted_iota(jnp.int32, (rows, pair), 1)
 
     for head in range(heads):
-        lam = lam_ref[mine_ref[0] * heads + head]
+        lam = lam_ref[place_ref[2] * heads + head]
         first_value = heads * pair + head * value_size
 
         for index, block in enumerate(blocks):
@@ -208,26 +243,28 @@
             value_ref[at, value_size:] = jnp.ones((keys, value_size), jnp.bfloat16)
 
         def step(following, score_to, peak_to, current, score_from, peak_from):
-            at = pl.ds(pl.multiple_of(following * rows, rows), rows)
-            q = q_ref[at, head * pair : (head + 1) * pair].astype(jnp.float32) * scale
-            q = jnp.concatenate(
-                [jnp.where(lanes < head_size, q, 0.0), jnp.where(lanes < head_size, 0.0, q)], axis=0
-            ).astype(jnp.bfloat16)
-            peak = jnp.full((2 * rows, 128), -jnp.inf, jnp.float32)
+            if following is not None:
+                at = pl.ds(pl.multiple_of(following * rows, rows), rows)
+                q = q_ref[at, head * pair : (head + 1) * pair].astype(jnp.float32) * scale
+                q = jnp.concatenate(
+                    [jnp.where(lanes < head_size, q, 0.0), jnp.where(lanes < head_size, 0.0, q)], axis=0
+                ).astype(jnp.bfloat16)
+                peak = jnp.full((2 * rows, 128), -jnp.inf, jnp.float32)
             if current is not None:
                 maxima = jnp.concatenate([peak_from[...]] * (keys // 128), axis=1)
                 total = jnp.zeros((2 * rows, 2 * value_size), jnp.float32)
             for index, block in enumerate(blocks):
                 columns = slice(index * keys, (index + 1) * keys)
-                scores = lax.dot_general(
-                    q,
-                    block[:, head * pair : (head + 1) * pair],
-                    (((1,), (1,)), ((), ())),
-                    preferred_element_type=jnp.float32,
-                )
-                score_to[:, columns] = scores
-                for part in range(keys // 128):
-                    peak = jnp.maximum(peak, scores[:, part * 128 : (part + 1) * 128])
+                if following is not None:
+                    scores = lax.dot_general(
+                        q,
+                        block[:, head * pair : (head + 1) * pair],
+                        (((1,), (1,)), ((), ())),
+                        preferred_element_type=jnp.float32,
+                    )
+                    score_to[:, columns] = scores
+                    for part in range(keys // 128):
+                        peak = jnp.maximum(peak, scores[:, part * 128 : (part + 1) * 128])
                 if current is not None:
                     weights = jnp.exp(score_from[:, columns] - maxima)
                     total = total + jnp.dot(
@@ -235,7 +272,8 @@
                         value_ref[columns, :],
                         preferred_element_type=jnp.float32,
                     )
-            peak_to[...] = jnp.broadcast_to(jnp.max(peak, axis=1, keepdims=True), peak.shape)
+            if following is not None:
+                peak_to[...] = jnp.broadcast_to(jnp.max(peak, axis=1, keepdims=True), peak.shape)
             if current is not None:
                 maps = total[:, :value_size] / total[:, value_size:]
                 head_out = maps[:rows] - lam * maps[rows:]
@@ -244,17 +282,19 @@
                 out_at = pl.ds(pl.multiple_of(current * rows, rows), rows)
                 out_ref[out_at, head * value_size : (head + 1) * value_size] = normal.astype(jnp.bfloat16)
 
-        step(0, score_a, peak_a, None, None, None)
-
         def two_tiles(i, carry):
             step(2 * i + 1, score_b, peak_b, 2 * i, score_a, peak_a)
-            step(jnp.minimum(2 * i + 2, tiles - 1), score_a, peak_a, 2 * i + 1, score_b, peak_b)
+            step(2 * i + 2, score_a, peak_a, 2 * i + 1, score_b, peak_b)
             return carry
 
-        lax.fori_loop(0, tiles // 2, two_tiles, 0)
-
-
-def attention(mine, lam, gain, q, blocks, heads):
+        step(0, score_a, peak_a, None, None, None)
+        if tiles > 2:
+            lax.fori_loop(0, tiles // 2 - 1, two_tiles, 0)
+        step(tiles - 1, score_b, peak_b, tiles - 2, score_a, peak_a)
+        step(None, None, None, tiles - 1, score_b, peak_b)
+
+
+def attention(place, lam, gain, q, blocks, heads):
     value_size = gain.shape[0]
     head_size = q.shape[1] // (2 * heads)
     queries = q.shape[0]
@@ -264,6 +304,8 @@
     while rows > 16 and 8 * rows * total_keys > 2**23:
         rows //= 2
     smem = pl.BlockSpec(memory_space=pltpu.SMEM)
+    scratch = 4 * total_keys * value_size + 16 * rows * (total_keys + 128)
+    room = scratch + 2 * blocks[0].size * len(blocks) + attention_margin
     return pl.pallas_call(
         functools.partial(attention_kernel, heads, head_size, value_size, rows, len(blocks)),
         out_shape=jax.ShapeDtypeStruct((queries, heads * value_size), jnp.bfloat16),
@@ -272,19 +314,19 @@
         scratch_shapes=[pltpu.VMEM((total_keys, 2 * value_size), jnp.bfloat16)]
         + [pltpu.VMEM((2 * rows, total_keys), jnp.float32)] * 2
         + [pltpu.VMEM((2 * rows, 128), jnp.float32)] * 2,
-        compiler_params=pltpu.CompilerParams(vmem_limit_bytes=attention_vmem),
+        compiler_params=pltpu.CompilerParams(vmem_limit_bytes=room),
         cost_estimate=pl.CostEstimate(
             flops=heads * queries * total_keys * 2 * 2 * (head_size + value_size) * 2,
             bytes_accessed=2 * total_keys * heads * (2 * head_size + value_size),
             transcendentals=2 * heads * queries * total_keys,
         ),
-    )(mine.reshape(1), lam, gain.reshape(1, -1), q, *blocks)
-
-
-def mixer_kernel(count, mine_ref, *refs):
+    )(place, lam, gain.reshape(1, -1), q, *blocks)
+
+
+def mixer_kernel(count, place_ref, *refs):
     columns, weights, out_ref = refs[:count], refs[count:-1], refs[-1]
     half = columns[0].shape[1] // 2
-    first = mine_ref[0] == 0
+    first = place_ref[2] == 0
     ordered = []
     for ref in columns:
         kept, other = ref[:, :half], ref[:, half:]
@@ -296,7 +338,7 @@
     ).astype(jnp.bfloat16)
 
 
-def mixer(mine, columns, weights):
+def mixer(place, columns, weights):
     rows, width = columns[0].shape[0], weights[0].shape[1]
     return pl.pallas_call(
         functools.partial(mixer_kernel, len(columns)),
@@ -310,17 +352,27 @@
             transcendentals=0,
         ),
         name="mixer",
-    )(mine.reshape(1), *columns, *weights)
-
-
-def gather_all(block, axis, size):
+    )(place, *columns, *weights)
+
+
+def gather_all(block, axis, bits):
     held = {0: block}
-    bit = size // 2
-    while bit:
+    for bit in bits:
         for index in list(held):
             held[index ^ bit] = swap(held[index], axis, bit)
-        bit //= 2
-    return [held[i] for i in range(size)]
+    return [held[i] for i in sorted(held)]
+
+
+def bits_below(size):
+    bits = []
+    while size > 1:
+        size //= 2
+        bits.append(size)
+    return bits
+
+
+def key_bits(ep):
+    return bits_below(ep)[:1] + bits_below(ep)[2:]
 
 
 def scatter_tp(stay, sent):
@@ -363,40 +415,21 @@
     tokens, top_count = routes.shape
     cap = capacity(tokens, top_count, ep)
 
-    hops = jnp.bitwise_xor(routes.T, me)
-    ranks, outgoing = dispatch(moe_input, moe_gain, hops, cap, ep)
+    partner = far // 2
+    place = jnp.stack([me, column, (me // partner) % 2]).astype(jnp.int32)
+    hops, ranks, outgoing = dispatch(place, moe_input, moe_gain, routes.T, cap, ep)
     ranks = window(ranks, expert_gate[0], expert_up[0], expert_down[0])
     quarter = ep // 4
     groups = [range(0, far), range(far, far + quarter), range(far + quarter, ep)]
 
     local_rows, local_heads = queries.shape[0], lambdas.shape[0]
     half = local_heads // 2
-    mine = (me // far).astype(jnp.int32)
-
-    def halves(array):
-        width = array.shape[1] // 2
-        first, second = array[:, :width], array[:, width:]
-        keep = jnp.where(mine == 0, first, second)
-        give = jnp.where(mine == 0, second, first)
-        return keep, give
-
+    kept, given, q_keep = pack(place, queries, key_rows, value_rows, tp)
+    came = swap(given, "ep", partner)
+    kv_width = kept.shape[1]
     parts = local_rows // tp
-    ordered = jnp.concatenate(
-        [
-            lax.dynamic_slice_in_dim(queries, jnp.bitwise_xor(column, b) * parts, parts, 0)
-            for b in range(tp)
-        ],
-        axis=0,
-    )
-    q_keep, q_give = halves(ordered)
-    k_keep, k_give = halves(key_rows)
-    v_keep, v_give = halves(value_rows)
-    kept = jnp.concatenate([k_keep, v_keep], axis=1)
-    given = jnp.concatenate([k_give, v_give, q_give], axis=1)
-    came = swap(given, "ep", far)
-    kv_width = kept.shape[1]
     came_kv, came_q = came[:, :kv_width], came[:, kv_width:]
-    key_blocks = gather_all(kept, "ep", far) + gather_all(came_kv, "ep", far)
+    key_blocks = gather_all(kept, "ep", key_bits(ep)) + gather_all(came_kv, "ep", key_bits(ep))
 
     arrived = {0: outgoing[0]}
     for group in (groups[1], groups[0], groups[2]):
@@ -404,21 +437,21 @@
             if k:
                 arrived[k] = swap(outgoing[k], "ep", k)
 
-    sent_out = attention(mine, lambdas, head_gain, came_q, key_blocks, half)
-    returned = swap(sent_out, "ep", far)
-    kept_out = attention(mine, lambdas, head_gain, q_keep, key_blocks, half)
+    sent_out = attention(place, lambdas, head_gain, came_q, key_blocks, half)
+    returned = swap(sent_out, "ep", partner)
+    kept_out = attention(place, lambdas, head_gain, q_keep, key_blocks, half)
     both = jnp.concatenate([kept_out, returned], axis=1)
     moved = [both[b * parts : (b + 1) * parts] for b in range(tp)]
     moved = [swap(block, "tp", b) if b else block for b, block in enumerate(moved)]
     half_rows = out_weight.shape[0] // 2
-    first_rows = gather_all(out_weight[:half_rows], "tp", tp)
-    last_rows = gather_all(out_weight[half_rows:], "tp", tp)
-    mixer_out = mixer(mine, moved, [w for pair in zip(first_rows, last_rows) for w in pair])
+    first_rows = gather_all(out_weight[:half_rows], "tp", bits_below(tp))
+    last_rows = gather_all(out_weight[half_rows:], "tp", bits_below(tp))
+    mixer_out = mixer(place, moved, [w for pair in zip(first_rows, last_rows) for w in pair])
 
     replies = {}
     for group in groups:
         block = jnp.concatenate([arrived[k] for k in group], axis=0)
-        blocks = gather_all(block, "tp", tp)
+        blocks = gather_all(block, "tp", bits_below(tp))
         partial = expert(blocks, expert_gate[0], expert_up[0], expert_down[0])
         summed = scatter_tp(partial[:-1], partial[-1])
         for index, k in enumerate(group):

time: 197 us -> 196 us (level)
  waiting for transfers between devices: 73.1 us -> 80.1 us
  Pallas kernels: 39.7 us -> 35.6 us
  local copies, waits for them, and re-layouts: 11.9 us -> 8.02 us
    ppermute x46, waiting for transfers between devices: 73.1 us -> 80.1 us  [swap(): return lax.ppermute(array, axis, [(i, i ^ mask) for i in range(size)])]
    pallas_call x2, Pallas kernels: 14.7 us -> 11.5 us  [attention(): pl.pallas_call(functools.partial(attention_kernel, heads, head_size, valu...]
    pallas_call x3, Pallas kernels: 21.2 us -> 18.5 us  [expert(): pl.pallas_call(functools.partial(expert_kernel, count), out_shape=shapes,...]
    unnamed x31 -> x33, local copies, waits for them, and re-layouts: 8.64 us -> 6.6 us
  transfers between devices with their start and end apart: 46 -> 46, of which waited for: 13 -> 18; matrix products, arithmetic and copies ran while one was open for 3% -> 1% of each run, Pallas kernels for 19% -> 17%
where the time goes in v1:
time: 196 us
  waiting for transfers between devices  80.1 us (41%)
  starting transfers between devices  69.7 us (36%)
  Pallas kernels  35.6 us (18%)
  local copies, waits for them, and re-layouts  8.02 us (4%)
    ppermute x46, waiting for transfers between devices, swap(): return lax.ppermute(array, axis, [(i, i ^ mask) for i in range(size)])  80.1 us
    ppermute x46, starting transfers between devices, swap(): return lax.ppermute(array, axis, [(i, i ^ mask) for i in range(size)])  69.7 us
    pallas_call x3, Pallas kernels, expert(): pl.pallas_call(functools.partial(expert_kernel, count), out_shape=shapes,...  18.5 us
    pallas_call x2, Pallas kernels, attention(): pl.pallas_call(functools.partial(attention_kernel, heads, head_size, valu...  11.5 us
    unnamed x33, local copies, waits for them, and re-layouts  6.6 us
  transfers between devices with their start and end apart: 46, of which 18 were waited for; matrix products, arithmetic and copies ran while one was open for 1% of the time, Pallas kernels for 17%

profile of v1, /device:TPU:0, one launch (start us, length us, event | category | flops | bytes accessed | tf_op | source)
XLA Modules:
  0.0 195.5 jit_solution(3765267834530799669)
XLA Ops:
  4.4 5.1 %collective-permute-start.37 = (bf16[40,2048]{1,0:T(8,128)(2,1)S(1)}, bf16[40,2048]{1,0:T(8,128)(2,1)S(1)}, u32[]{:S(2)}, u32[]{:S(2)}) collective-permute-start(bf16[40,2048]{1,0:T(8,128)(2,1)S(1)} %get-tuple-element.41), channel_id=1, source_target_pairs={{0,24},{4,28},{8,16},{12,20},{16,8},{20,12},{24,0},{28,4},{1,25},{... | collective-permute-start | bytes 491528 | tf_op jit(solution)/shard_map/ppermute | solution.py:27
  11.5 1.9 collective-permute-start.29
  13.4 1.7 collective-permute-start.17
  17.1 11.3 %collective-permute-start.18 = (bf16[40,2048]{1,0:T(8,128)(2,1)S(1)}, bf16[40,2048]{1,0:T(8,128)(2,1)S(1)}, u32[]{:S(2)}, u32[]{:S(2)}) collective-permute-start(bf16[40,2048]{1,0:T(8,128)(2,1)S(1)} %get-tuple-element.31), channel_id=1, source_target_pairs={{0,8},{4,12},{8,0},{12,4},{16,24},{20,28},{24,16},{28,20},{1,9},{5... | collective-permute-start | bytes 491528 | tf_op jit(solution)/shard_map/ppermute | solution.py:27
  28.4 6.5 %collective-permute-done.28 = bf16[40,2048]{1,0:T(8,128)(2,1)S(1)} collective-permute-done((bf16[40,2048]{1,0:T(8,128)(2,1)S(1)}, bf16[40,2048]{1,0:T(8,128)(2,1)S(1)}, u32[]{:S(2)}, u32[]{:S(2)}) %collective-permute-start.28) | collective-permute-done | bytes 163872 | tf_op jit(solution)/shard_map/ppermute | solution.py:27
  35.8 2.3 %collective-permute-start.3 = (bf16[512,384]{1,0:T(8,128)(2,1)S(1)}, bf16[512,384]{1,0:T(8,128)(2,1)S(1)}, u32[]{:S(2)}, u32[]{:S(2)}) collective-permute-start(bf16[512,384]{1,0:T(8,128)(2,1)S(1)} %get-tuple-element.26), channel_id=1, source_target_pairs={{0,8},{4,12},{8,0},{12,4},{16,24},{20,28},{24,16},{28,20},{1,9},{5... | collective-permute-start | bytes 1179656 | tf_op jit(solution)/shard_map/ppermute | solution.py:27
  40.9 8.1 %collective-permute-done.40.refs_2_ = bf16[80,2048]{1,0:T(8,128)(2,1)S(1)} collective-permute-done((bf16[80,2048]{1,0:T(8,128)(2,1)S(1)}, bf16[80,2048]{1,0:T(8,128)(2,1)S(1)}, u32[]{:S(2)}, u32[]{:S(2)}) %collective-permute-start.40) | collective-permute-done | bytes 327712 | tf_op jit(solution)/shard_map/ppermute | solution.py:27
  52.1 2.8 %collective-permute-done.31.refs_2_ = bf16[80,2048]{1,0:T(8,128)(2,1)S(1)} collective-permute-done((bf16[80,2048]{1,0:T(8,128)(2,1)S(1)}, bf16[80,2048]{1,0:T(8,128)(2,1)S(1)}, u32[]{:S(2)}, u32[]{:S(2)}) %collective-permute-start.31) | collective-permute-done | bytes 327712 | tf_op jit(solution)/shard_map/ppermute | solution.py:27
  54.9 2.0 %copy-done.1 = bf16[1,2048,896]{2,1,0:T(8,128)(2,1)S(1)} copy-done((bf16[1,2048,896]{2,1,0:T(8,128)(2,1)S(1)}, bf16[1,2048,896]{2,1,0:T(8,128)(2,1)}, u32[]{:S(2)}) %copy-start.1) | copy-done | bytes 3670040
  56.9 2.0 %copy-done.3 = bf16[1,896,2048]{2,1,0:T(8,128)(2,1)S(1)} copy-done((bf16[1,896,2048]{2,1,0:T(8,128)(2,1)S(1)}, bf16[1,896,2048]{2,1,0:T(8,128)(2,1)}, u32[]{:S(2)}) %copy-start.3) | copy-done | bytes 3670040
  59.0 4.5 %shard_map.144 = (bf16[80,2048]{1,0:T(8,128)(2,1)S(1)}, bf16[80,2048]{1,0:T(8,128)(2,1)S(1)}, bf16[160,2048]{1,0:T(8,128)(2,1)S(1)}) custom-call(bf16[80,2048]{1,0:T(8,128)(2,1)S(1)} %constant_dynamic-update-slice_fusion.6.refs_0_, bf16[80,2048]{1,0:T(8,128)(2,1)S(1)} %collective-permute-done.39.refs_1_, ...), custom_call_target="tpu_custom_call" | custom-call | flops 3523215360 | bytes 13631488 | tf_op jit(solution)/shard_map/pallas_call | solution.py:212
  63.5 6.4 %collective-permute-done.1.refs_2_ = bf16[512,256]{1,0:T(8,128)(2,1)S(1)} collective-permute-done((bf16[512,256]{1,0:T(8,128)(2,1)S(1)}, bf16[512,256]{1,0:T(8,128)(2,1)S(1)}, u32[]{:S(2)}, u32[]{:S(2)}) %collective-permute-start.1) | collective-permute-done | bytes 262176 | tf_op jit(solution)/shard_map/ppermute | solution.py:27
  72.0 3.5 %collective-permute-done.5.refs_6_ = bf16[512,256]{1,0:T(8,128)(2,1)S(1)} collective-permute-done((bf16[512,256]{1,0:T(8,128)(2,1)S(1)}, bf16[512,256]{1,0:T(8,128)(2,1)S(1)}, u32[]{:S(2)}, u32[]{:S(2)}) %collective-permute-start.5) | collective-permute-done | bytes 262176 | tf_op jit(solution)/shard_map/ppermute | solution.py:27
  77.5 4.5 %shard_map.143 = (bf16[80,2048]{1,0:T(8,128)(2,1)S(1)}, bf16[80,2048]{1,0:T(8,128)(2,1)S(1)}, bf16[160,2048]{1,0:T(8,128)(2,1)S(1)}) custom-call(bf16[80,2048]{1,0:T(8,128)(2,1)S(1)} %constant_dynamic-update-slice_fusion.4.refs_0_, bf16[80,2048]{1,0:T(8,128)(2,1)S(1)} %collective-permute-done.30.refs_1_, ...), custom_call_target="tpu_custom_call" | custom-call | flops 3523215360 | bytes 13631488 | tf_op jit(solution)/shard_map/pallas_call | solution.py:212
  84.7 5.6 %collective-permute-done.4.refs_5_ = bf16[512,256]{1,0:T(8,128)(2,1)S(1)} collective-permute-done((bf16[512,256]{1,0:T(8,128)(2,1)S(1)}, bf16[512,256]{1,0:T(8,128)(2,1)S(1)}, u32[]{:S(2)}, u32[]{:S(2)}) %collective-permute-start.4) | collective-permute-done | bytes 262176 | tf_op jit(solution)/shard_map/ppermute | solution.py:27
  90.8 4.2 %collective-permute-done.6.refs_7_ = bf16[512,256]{1,0:T(8,128)(2,1)S(1)} collective-permute-done((bf16[512,256]{1,0:T(8,128)(2,1)S(1)}, bf16[512,256]{1,0:T(8,128)(2,1)S(1)}, u32[]{:S(2)}, u32[]{:S(2)}) %collective-permute-start.6) | collective-permute-done | bytes 262176 | tf_op jit(solution)/shard_map/ppermute | solution.py:27
  95.0 5.8 %shard_map.141 = bf16[512,128]{1,0:T(8,128)(2,1)S(1)} custom-call(s32[3]{0:T(128)S(1)} %pad_add_fusion.place_ref, f32[2]{0:T(128)S(1)} %copy-done.12, f32[1,128]{1,0:T(1,128)S(1)} %bitcast.25, bf16[512,128]{1,0:T(8,128)(2,1)S(1)} %slice.89.q_ref, bf16[512,256]{1,0:T(8,128)(2,1)S(1)} %get-tuple-element.25.refs_0_, ...), custom_call_target="tpu_custom_call" | custom-call | flops 3221225472 | bytes 2097152 | tf_op jit(solution)/shard_map/pallas_call | solution.py:309
  101.0 5.7 %shard_map.140 = bf16[512,128]{1,0:T(8,128)(2,1)S(1)} custom-call(s32[3]{0:T(128)S(1)} %pad_add_fusion.place_ref, f32[2]{0:T(128)S(1)} %copy-done.12, f32[1,128]{1,0:T(1,128)S(1)} %bitcast.26, bf16[512,128]{1,0:T(8,128)(2,1)S(1)} %get-tuple-element.24.q_ref, bf16[512,256]{1,0:T(8,128)(2,1)S(1)} %get-tuple-element.25.refs_0_, ...), custom_call_target="tpu_custom_call" | custom-call | flops 3221225472 | bytes 2097152 | tf_op jit(solution)/shard_map/pallas_call | solution.py:309
  109.3 9.5 %shard_map.142 = (bf16[160,2048]{1,0:T(8,128)(2,1)S(1)}, bf16[160,2048]{1,0:T(8,128)(2,1)S(1)}, bf16[320,2048]{1,0:T(8,128)(2,1)S(1)}) custom-call(bf16[160,2048]{1,0:T(8,128)(2,1)S(1)} %constant_dynamic-update-slice_fusion.refs_0_, bf16[160,2048]{1,0:T(8,128)(2,1)S(1)} %collective-permute-done.20.refs_1_, ...), custom_call_target="tpu_custom_call" | custom-call | flops 7046430720 | bytes 16252928 | tf_op jit(solution)/shard_map/pallas_call | solution.py:212
  118.9 9.2 %collective-permute-done.43 = bf16[80,2048]{1,0:T(8,128)(2,1)S(1)} collective-permute-done((bf16[80,2048]{1,0:T(8,128)(2,1)S(1)}, bf16[80,2048]{1,0:T(8,128)(2,1)S(1)}, u32[]{:S(2)}, u32[]{:S(2)}) %collective-permute-start.43) | collective-permute-done | bytes 327712 | tf_op jit(solution)/shard_map/ppermute | solution.py:27
  130.4 7.0 %collective-permute-done.34 = bf16[80,2048]{1,0:T(8,128)(2,1)S(1)} collective-permute-done((bf16[80,2048]{1,0:T(8,128)(2,1)S(1)}, bf16[80,2048]{1,0:T(8,128)(2,1)S(1)}, u32[]{:S(2)}, u32[]{:S(2)}) %collective-permute-start.34) | collective-permute-done | bytes 327712 | tf_op jit(solution)/shard_map/ppermute | solution.py:27
  139.4 15.6 %collective-permute-done.24 = bf16[160,2048]{1,0:T(8,128)(2,1)S(1)} collective-permute-done((bf16[160,2048]{1,0:T(8,128)(2,1)S(1)}, bf16[160,2048]{1,0:T(8,128)(2,1)S(1)}, u32[]{:S(2)}, u32[]{:S(2)}) %collective-permute-start.24) | collective-permute-done | bytes 655392 | tf_op jit(solution)/shard_map/ppermute | solution.py:27
  157.5 1.7 collective-permute-start.44
  159.2 2.1 %collective-permute-start.45 = (bf16[40,2048]{1,0:T(8,128)(2,1)S(1)}, bf16[40,2048]{1,0:T(8,128)(2,1)S(1)}, u32[]{:S(2)}, u32[]{:S(2)}) collective-permute-start(bf16[40,2048]{1,0:T(8,128)(2,1)S(1)} %get-tuple-element.52), channel_id=1, source_target_pairs={{0,28},{4,24},{8,20},{12,16},{16,12},{20,8},{24,4},{28,0},{1,29},{... | collective-permute-start | bytes 491528 | tf_op jit(solution)/shard_map/ppermute | solution.py:27
  162.1 3.2 %collective-permute-start.36 = (bf16[40,2048]{1,0:T(8,128)(2,1)S(1)}, bf16[40,2048]{1,0:T(8,128)(2,1)S(1)}, u32[]{:S(2)}, u32[]{:S(2)}) collective-permute-start(bf16[40,2048]{1,0:T(8,128)(2,1)S(1)} %get-tuple-element.54), channel_id=1, source_target_pairs={{0,20},{4,16},{8,28},{12,24},{16,4},{20,0},{24,12},{28,8},{1,21},{... | collective-permute-start | bytes 491528 | tf_op jit(solution)/shard_map/ppermute | solution.py:27
  166.5 13.5 %collective-permute-start.26 = (bf16[40,2048]{1,0:T(8,128)(2,1)S(1)}, bf16[40,2048]{1,0:T(8,128)(2,1)S(1)}, u32[]{:S(2)}, u32[]{:S(2)}) collective-permute-start(bf16[40,2048]{1,0:T(8,128)(2,1)S(1)} %get-tuple-element.49), channel_id=1, source_target_pairs={{0,8},{4,12},{8,0},{12,4},{16,24},{20,28},{24,16},{28,20},{1,9},{5... | collective-permute-start | bytes 491528 | tf_op jit(solution)/shard_map/ppermute | solution.py:27
  180.0 4.4 %collective-permute-start.27 = (bf16[40,2048]{1,0:T(8,128)(2,1)S(1)}, bf16[40,2048]{1,0:T(8,128)(2,1)S(1)}, u32[]{:S(2)}, u32[]{:S(2)}) collective-permute-start(bf16[40,2048]{1,0:T(8,128)(2,1)S(1)} %get-tuple-element.48), channel_id=1, source_target_pairs={{0,12},{4,8},{8,4},{12,0},{16,28},{20,24},{24,20},{28,16},{1,13},{... | collective-permute-start | bytes 491528 | tf_op jit(solution)/shard_map/ppermute | solution.py:27
  184.4 2.1 %mixer.1 = bf16[128,2048]{1,0:T(8,128)(2,1)} custom-call(s32[3]{0:T(128)S(1)} %pad_add_fusion.place_ref, bf16[128,256]{1,0:T(8,128)(2,1)S(1)} %get-tuple-element.57.refs_0_, bf16[128,256]{1,0:T(8,128)(2,1)S(1)} %collective-permute-done.8.refs_1_, bf16[128,256]{1,0:T(8,128)(2,1)S(1)} %collective-permute-done.9.refs_2_, ...), custom_call_target="tpu_custom_call" | custom-call | flops 536870912 | bytes 4194304 | tf_op jit(solution)/shard_map/mixer/pallas_call | solution.py:343
  186.5 3.0 %collective-permute-done.36.refs_5_ = bf16[40,2048]{1,0:T(8,128)(2,1)S(1)} collective-permute-done((bf16[40,2048]{1,0:T(8,128)(2,1)S(1)}, bf16[40,2048]{1,0:T(8,128)(2,1)S(1)}, u32[]{:S(2)}, u32[]{:S(2)}) %collective-permute-start.36) | collective-permute-done | bytes 163872 | tf_op jit(solution)/shard_map/ppermute | solution.py:27
  189.5 2.0 collective-permute-done.26.refs_2_
  191.5 2.5 %collective-permute-done.27.refs_3_ = bf16[40,2048]{1,0:T(8,128)(2,1)S(1)} collective-permute-done((bf16[40,2048]{1,0:T(8,128)(2,1)S(1)}, bf16[40,2048]{1,0:T(8,128)(2,1)S(1)}, u32[]{:S(2)}, u32[]{:S(2)}) %collective-permute-start.27) | collective-permute-done | bytes 163872 | tf_op jit(solution)/shard_map/ppermute | solution.py:27
  194.0 1.6 combine.1
  (120 shorter events, 32.9 us)
Async XLA Ops:
  9.5 26.2 %collective-permute-start.38 = (bf16[40,2048]{1,0:T(8,128)(2,1)S(1)}, bf16[40,2048]{1,0:T(8,128)(2,1)S(1)}, u32[]{:S(2)}, u32[]{:S(2)}) collective-permute-start(bf16[40,2048]{1,0:T(8,128)(2,1)S(1)} %get-tuple-element.42), channel_id=1, source_target_pairs={{0,28},{4,24},{8,20},{12,16},{16,12},{20,8},{24,4},{28,0},{1,29},{... | collective-permute-start | bytes 491528 | tf_op jit(solution)/shard_map/ppermute | solution.py:27
  10.7 24.3 %collective-permute-start.28 = (bf16[40,2048]{1,0:T(8,128)(2,1)S(1)}, bf16[40,2048]{1,0:T(8,128)(2,1)S(1)}, u32[]{:S(2)}, u32[]{:S(2)}) collective-permute-start(bf16[40,2048]{1,0:T(8,128)(2,1)S(1)} %get-tuple-element.36), channel_id=1, source_target_pairs={{0,16},{4,20},{8,24},{12,28},{16,0},{20,4},{24,8},{28,12},{1,17},{... | collective-permute-start | bytes 491528 | tf_op jit(solution)/shard_map/ppermute | solution.py:27
  11.5 27.0 %collective-permute-start.29 = (bf16[40,2048]{1,0:T(8,128)(2,1)S(1)}, bf16[40,2048]{1,0:T(8,128)(2,1)S(1)}, u32[]{:S(2)}, u32[]{:S(2)}) collective-permute-start(bf16[40,2048]{1,0:T(8,128)(2,1)S(1)} %get-tuple-element.37), channel_id=1, source_target_pairs={{0,20},{4,16},{8,28},{12,24},{16,4},{20,0},{24,12},{28,8},{1,21},{... | collective-permute-start | bytes 491528 | tf_op jit(solution)/shard_map/ppermute | solution.py:27
  13.4 26.6 %collective-permute-start.17 = (bf16[40,2048]{1,0:T(8,128)(2,1)S(1)}, bf16[40,2048]{1,0:T(8,128)(2,1)S(1)}, u32[]{:S(2)}, u32[]{:S(2)}) collective-permute-start(bf16[40,2048]{1,0:T(8,128)(2,1)S(1)} %get-tuple-element.30), channel_id=1, source_target_pairs={{0,4},{4,0},{8,12},{12,8},{16,20},{20,16},{24,28},{28,24},{1,5},{5... | collective-permute-start | bytes 491528 | tf_op jit(solution)/shard_map/ppermute | solution.py:27
  17.1 23.0 %collective-permute-start.18 = (bf16[40,2048]{1,0:T(8,128)(2,1)S(1)}, bf16[40,2048]{1,0:T(8,128)(2,1)S(1)}, u32[]{:S(2)}, u32[]{:S(2)}) collective-permute-start(bf16[40,2048]{1,0:T(8,128)(2,1)S(1)} %get-tuple-element.31), channel_id=1, source_target_pairs={{0,8},{4,12},{8,0},{12,4},{16,24},{20,28},{24,16},{28,20},{1,9},{5... | collective-permute-start | bytes 491528 | tf_op jit(solution)/shard_map/ppermute | solution.py:27
  35.8 14.7 %collective-permute-start.3 = (bf16[512,384]{1,0:T(8,128)(2,1)S(1)}, bf16[512,384]{1,0:T(8,128)(2,1)S(1)}, u32[]{:S(2)}, u32[]{:S(2)}) collective-permute-start(bf16[512,384]{1,0:T(8,128)(2,1)S(1)} %get-tuple-element.26), channel_id=1, source_target_pairs={{0,8},{4,12},{8,0},{12,4},{16,24},{20,28},{24,16},{28,20},{1,9},{5... | collective-permute-start | bytes 1179656 | tf_op jit(solution)/shard_map/ppermute | solution.py:27
  40.1 14.7 %collective-permute-start.31 = (bf16[80,2048]{1,0:T(8,128)(2,1)S(1)}, bf16[80,2048]{1,0:T(8,128)(2,1)S(1)}, u32[]{:S(2)}, u32[]{:S(2)}) collective-permute-start(bf16[80,2048]{1,0:T(8,128)(2,1)S(1)} %constant_dynamic-update-slice_fusion.4.refs_0_), channel_id=1, source_target_pairs={{0,2},{1,3},{2,0},{3,1},{4,6},{5,7},{6,4},{7,5},{8,10},{9,11},{10,... | collective-permute-start | bytes 983048 | tf_op jit(solution)/shard_map/ppermute | solution.py:27
  49.1 20.8 %collective-permute-start.1 = (bf16[512,256]{1,0:T(8,128)(2,1)S(1)}, bf16[512,256]{1,0:T(8,128)(2,1)S(1)}, u32[]{:S(2)}, u32[]{:S(2)}) collective-permute-start(bf16[512,256]{1,0:T(8,128)(2,1)S(1)} %get-tuple-element.25.refs_0_), channel_id=1, source_target_pairs={{0,16},{4,20},{8,24},{12,28},{16,0},{20,4},{24,8},{28,12},{1,17},{... | collective-permute-start | bytes 786440 | tf_op jit(solution)/shard_map/ppermute | solution.py:27
  50.4 20.0 %collective-permute-start.30 = (bf16[80,2048]{1,0:T(8,128)(2,1)S(1)}, bf16[80,2048]{1,0:T(8,128)(2,1)S(1)}, u32[]{:S(2)}, u32[]{:S(2)}) collective-permute-start(bf16[80,2048]{1,0:T(8,128)(2,1)S(1)} %constant_dynamic-update-slice_fusion.4.refs_0_), channel_id=1, source_target_pairs={{0,1},{1,0},{2,3},{3,2},{4,5},{5,4},{6,7},{7,6},{8,9},{9,8},{10,11... | collective-permute-start | bytes 983048 | tf_op jit(solution)/shard_map/ppermute | solution.py:27
  50.5 39.8 %collective-permute-start.21 = (bf16[160,2048]{1,0:T(8,128)(2,1)S(1)}, bf16[160,2048]{1,0:T(8,128)(2,1)S(1)}, u32[]{:S(2)}, u32[]{:S(2)}) collective-permute-start(bf16[160,2048]{1,0:T(8,128)(2,1)S(1)} %constant_dynamic-update-slice_fusion.refs_0_), channel_id=1, source_target_pairs={{0,2},{1,3},{2,0},{3,1},{4,6},{5,7},{6,4},{7,5},{8,10},{9,11},{10,... | collective-permute-start | bytes 1966088 | tf_op jit(solution)/shard_map/ppermute | solution.py:27
  54.9 20.6 %collective-permute-start.5 = (bf16[512,256]{1,0:T(8,128)(2,1)S(1)}, bf16[512,256]{1,0:T(8,128)(2,1)S(1)}, u32[]{:S(2)}, u32[]{:S(2)}) collective-permute-start(bf16[512,256]{1,0:T(8,128)(2,1)S(1)} %slice.88.refs_4_), channel_id=1, source_target_pairs={{0,16},{4,20},{8,24},{12,28},{16,0},{20,4},{24,8},{28,12},{1,17},{... | collective-permute-start | bytes 786440 | tf_op jit(solution)/shard_map/ppermute | solution.py:27
  54.9 21.1 %collective-permute-start.32 = (bf16[80,2048]{1,0:T(8,128)(2,1)S(1)}, bf16[80,2048]{1,0:T(8,128)(2,1)S(1)}, u32[]{:S(2)}, u32[]{:S(2)}) collective-permute-start(bf16[80,2048]{1,0:T(8,128)(2,1)S(1)} %collective-permute-done.31.refs_2_), channel_id=1, source_target_pairs={{0,1},{1,0},{2,3},{3,2},{4,5},{5,4},{6,7},{7,6},{8,9},{9,8},{10,11... | collective-permute-start | bytes 983048 | tf_op jit(solution)/shard_map/ppermute | solution.py:27
  70.4 14.3 %collective-permute-start.2 = (bf16[512,256]{1,0:T(8,128)(2,1)S(1)}, bf16[512,256]{1,0:T(8,128)(2,1)S(1)}, u32[]{:S(2)}, u32[]{:S(2)}) collective-permute-start(bf16[512,256]{1,0:T(8,128)(2,1)S(1)} %collective-permute-done.1.refs_2_), channel_id=1, source_target_pairs={{0,4},{4,0},{8,12},{12,8},{16,20},{20,16},{24,28},{28,24},{1,5},{5... | collective-permute-start | bytes 786440 | tf_op jit(solution)/shard_map/ppermute | solution.py:27
  75.5 14.8 %collective-permute-start.4 = (bf16[512,256]{1,0:T(8,128)(2,1)S(1)}, bf16[512,256]{1,0:T(8,128)(2,1)S(1)}, u32[]{:S(2)}, u32[]{:S(2)}) collective-permute-start(bf16[512,256]{1,0:T(8,128)(2,1)S(1)} %slice.88.refs_4_), channel_id=1, source_target_pairs={{0,4},{4,0},{8,12},{12,8},{16,20},{20,16},{24,28},{28,24},{1,5},{5... | collective-permute-start | bytes 786440 | tf_op jit(solution)/shard_map/ppermute | solution.py:27
  76.0 19.0 %collective-permute-start.6 = (bf16[512,256]{1,0:T(8,128)(2,1)S(1)}, bf16[512,256]{1,0:T(8,128)(2,1)S(1)}, u32[]{:S(2)}, u32[]{:S(2)}) collective-permute-start(bf16[512,256]{1,0:T(8,128)(2,1)S(1)} %collective-permute-done.5.refs_6_), channel_id=1, source_target_pairs={{0,4},{4,0},{8,12},{12,8},{16,20},{20,16},{24,28},{28,24},{1,5},{5... | collective-permute-start | bytes 786440 | tf_op jit(solution)/shard_map/ppermute | solution.py:27
  82.1 47.7 %collective-permute-start.13 = (bf16[128,2048]{1,0:T(8,128)(2,1)S(1)}, bf16[128,2048]{1,0:T(8,128)(2,1)S(1)}, u32[]{:S(2)}, u32[]{:S(2)}) collective-permute-start(bf16[128,2048]{1,0:T(8,128)(2,1)S(1)} %get-tuple-element.47.refs_4_), channel_id=1, source_target_pairs={{0,2},{1,3},{2,0},{3,1},{4,6},{5,7},{6,4},{7,5},{8,10},{9,11},{10,... | collective-permute-start | bytes 1572872 | tf_op jit(solution)/shard_map/ppermute | solution.py:27
  84.7 23.7 %collective-permute-start.20 = (bf16[160,2048]{1,0:T(8,128)(2,1)S(1)}, bf16[160,2048]{1,0:T(8,128)(2,1)S(1)}, u32[]{:S(2)}, u32[]{:S(2)}) collective-permute-start(bf16[160,2048]{1,0:T(8,128)(2,1)S(1)} %constant_dynamic-update-slice_fusion.refs_0_), channel_id=1, source_target_pairs={{0,1},{1,0},{2,3},{3,2},{4,5},{5,4},{6,7},{7,6},{8,9},{9,8},{10,11... | collective-permute-start | bytes 1966088 | tf_op jit(solution)/shard_map/ppermute | solution.py:27
  90.3 16.4 %collective-permute-start.42 = (bf16[160,2048]{1,0:T(8,128)(2,1)S(1)}, bf16[160,2048]{1,0:T(8,128)(2,1)S(1)}, u32[]{:S(2)}, u32[]{:S(2)}) collective-permute-start(bf16[160,2048]{1,0:T(8,128)(2,1)S(1)} %get-tuple-element.44), channel_id=1, source_target_pairs={{0,1},{1,0},{2,3},{3,2},{4,5},{5,4},{6,7},{7,6},{8,9},{9,8},{10,11... | collective-permute-start | bytes 1966088 | tf_op jit(solution)/shard_map/ppermute | solution.py:27
  90.3 18.4 %collective-permute-start.22 = (bf16[160,2048]{1,0:T(8,128)(2,1)S(1)}, bf16[160,2048]{1,0:T(8,128)(2,1)S(1)}, u32[]{:S(2)}, u32[]{:S(2)}) collective-permute-start(bf16[160,2048]{1,0:T(8,128)(2,1)S(1)} %collective-permute-done.21.refs_2_), channel_id=1, source_target_pairs={{0,1},{1,0},{2,3},{3,2},{4,5},{5,4},{6,7},{7,6},{8,9},{9,8},{10,11... | collective-permute-start | bytes 1966088 | tf_op jit(solution)/shard_map/ppermute | solution.py:27
  106.6 49.4 %collective-permute-start.11 = (bf16[128,2048]{1,0:T(8,128)(2,1)S(1)}, bf16[128,2048]{1,0:T(8,128)(2,1)S(1)}, u32[]{:S(2)}, u32[]{:S(2)}) collective-permute-start(bf16[128,2048]{1,0:T(8,128)(2,1)S(1)} %get-tuple-element.47.refs_4_), channel_id=1, source_target_pairs={{0,1},{1,0},{2,3},{3,2},{4,5},{5,4},{6,7},{7,6},{8,9},{9,8},{10,11... | collective-permute-start | bytes 1572872 | tf_op jit(solution)/shard_map/ppermute | solution.py:27
  106.8 23.1 %collective-permute-start.14 = (bf16[128,2048]{1,0:T(8,128)(2,1)S(1)}, bf16[128,2048]{1,0:T(8,128)(2,1)S(1)}, u32[]{:S(2)}, u32[]{:S(2)}) collective-permute-start(bf16[128,2048]{1,0:T(8,128)(2,1)S(1)} %get-tuple-element.46.refs_5_), channel_id=1, source_target_pairs={{0,2},{1,3},{2,0},{3,1},{4,6},{5,7},{6,4},{7,5},{8,10},{9,11},{10,... | collective-permute-start | bytes 1572872 | tf_op jit(solution)/shard_map/ppermute | solution.py:27
  108.7 19.5 %collective-permute-start.43 = (bf16[80,2048]{1,0:T(8,128)(2,1)S(1)}, bf16[80,2048]{1,0:T(8,128)(2,1)S(1)}, u32[]{:S(2)}, u32[]{:S(2)}) collective-permute-start(bf16[80,2048]{1,0:T(8,128)(2,1)S(1)} %add_convert_fusion.4), channel_id=1, source_target_pairs={{0,2},{1,3},{2,0},{3,1},{4,6},{5,7},{6,4},{7,5},{8,10},{9,11},{10,... | collective-permute-start | bytes 983048 | tf_op jit(solution)/shard_map/ppermute | solution.py:27
  118.8 18.8 %collective-permute-start.23 = (bf16[320,2048]{1,0:T(8,128)(2,1)S(1)}, bf16[320,2048]{1,0:T(8,128)(2,1)S(1)}, u32[]{:S(2)}, u32[]{:S(2)}) collective-permute-start(bf16[320,2048]{1,0:T(8,128)(2,1)S(1)} %get-tuple-element.34), channel_id=1, source_target_pairs={{0,1},{1,0},{2,3},{3,2},{4,5},{5,4},{6,7},{7,6},{8,9},{9,8},{10,11... | collective-permute-start | bytes 3932168 | tf_op jit(solution)/shard_map/ppermute | solution.py:27
  129.8 27.2 %collective-permute-start.12 = (bf16[128,2048]{1,0:T(8,128)(2,1)S(1)}, bf16[128,2048]{1,0:T(8,128)(2,1)S(1)}, u32[]{:S(2)}, u32[]{:S(2)}) collective-permute-start(bf16[128,2048]{1,0:T(8,128)(2,1)S(1)} %get-tuple-element.46.refs_5_), channel_id=1, source_target_pairs={{0,1},{1,0},{2,3},{3,2},{4,5},{5,4},{6,7},{7,6},{8,9},{9,8},{10,11... | collective-permute-start | bytes 1572872 | tf_op jit(solution)/shard_map/ppermute | solution.py:27
  129.9 27.6 %collective-permute-start.15 = (bf16[128,2048]{1,0:T(8,128)(2,1)S(1)}, bf16[128,2048]{1,0:T(8,128)(2,1)S(1)}, u32[]{:S(2)}, u32[]{:S(2)}) collective-permute-start(bf16[128,2048]{1,0:T(8,128)(2,1)S(1)} %collective-permute-done.13.refs_8_), channel_id=1, source_target_pairs={{0,1},{1,0},{2,3},{3,2},{4,5},{5,4},{6,7},{7,6},{8,9},{9,8},{10,11... | collective-permute-start | bytes 1572872 | tf_op jit(solution)/shard_map/ppermute | solution.py:27
  137.4 21.8 %collective-permute-start.16 = (bf16[128,2048]{1,0:T(8,128)(2,1)S(1)}, bf16[128,2048]{1,0:T(8,128)(2,1)S(1)}, u32[]{:S(2)}, u32[]{:S(2)}) collective-permute-start(bf16[128,2048]{1,0:T(8,128)(2,1)S(1)} %collective-permute-done.14.refs_9_), channel_id=1, source_target_pairs={{0,1},{1,0},{2,3},{3,2},{4,5},{5,4},{6,7},{7,6},{8,9},{9,8},{10,11... | collective-permute-start | bytes 1572872 | tf_op jit(solution)/shard_map/ppermute | solution.py:27
  137.8 17.2 %collective-permute-start.24 = (bf16[160,2048]{1,0:T(8,128)(2,1)S(1)}, bf16[160,2048]{1,0:T(8,128)(2,1)S(1)}, u32[]{:S(2)}, u32[]{:S(2)}) collective-permute-start(bf16[160,2048]{1,0:T(8,128)(2,1)S(1)} %add_convert_fusion.1), channel_id=1, source_target_pairs={{0,2},{1,3},{2,0},{3,1},{4,6},{5,7},{6,4},{7,5},{8,10},{9,11},{10,... | collective-permute-start | bytes 1966088 | tf_op jit(solution)/shard_map/ppermute | solution.py:27
  159.2 20.7 %collective-permute-start.45 = (bf16[40,2048]{1,0:T(8,128)(2,1)S(1)}, bf16[40,2048]{1,0:T(8,128)(2,1)S(1)}, u32[]{:S(2)}, u32[]{:S(2)}) collective-permute-start(bf16[40,2048]{1,0:T(8,128)(2,1)S(1)} %get-tuple-element.52), channel_id=1, source_target_pairs={{0,28},{4,24},{8,20},{12,16},{16,12},{20,8},{24,4},{28,0},{1,29},{... | collective-permute-start | bytes 491528 | tf_op jit(solution)/shard_map/ppermute | solution.py:27
  161.4 25.1 %collective-permute-start.35 = (bf16[40,2048]{1,0:T(8,128)(2,1)S(1)}, bf16[40,2048]{1,0:T(8,128)(2,1)S(1)}, u32[]{:S(2)}, u32[]{:S(2)}) collective-permute-start(bf16[40,2048]{1,0:T(8,128)(2,1)S(1)} %get-tuple-element.55), channel_id=1, source_target_pairs={{0,16},{4,20},{8,24},{12,28},{16,0},{20,4},{24,8},{28,12},{1,17},{... | collective-permute-start | bytes 491528 | tf_op jit(solution)/shard_map/ppermute | solution.py:27
  162.1 27.4 %collective-permute-start.36 = (bf16[40,2048]{1,0:T(8,128)(2,1)S(1)}, bf16[40,2048]{1,0:T(8,128)(2,1)S(1)}, u32[]{:S(2)}, u32[]{:S(2)}) collective-permute-start(bf16[40,2048]{1,0:T(8,128)(2,1)S(1)} %get-tuple-element.54), channel_id=1, source_target_pairs={{0,20},{4,16},{8,28},{12,24},{16,4},{20,0},{24,12},{28,8},{1,21},{... | collective-permute-start | bytes 491528 | tf_op jit(solution)/shard_map/ppermute | solution.py:27
  165.3 24.2 %collective-permute-start.25 = (bf16[40,2048]{1,0:T(8,128)(2,1)S(1)}, bf16[40,2048]{1,0:T(8,128)(2,1)S(1)}, u32[]{:S(2)}, u32[]{:S(2)}) collective-permute-start(bf16[40,2048]{1,0:T(8,128)(2,1)S(1)} %get-tuple-element.50), channel_id=1, source_target_pairs={{0,4},{4,0},{8,12},{12,8},{16,20},{20,16},{24,28},{28,24},{1,5},{5... | collective-permute-start | bytes 491528 | tf_op jit(solution)/shard_map/ppermute | solution.py:27
  166.5 25.0 %collective-permute-start.26 = (bf16[40,2048]{1,0:T(8,128)(2,1)S(1)}, bf16[40,2048]{1,0:T(8,128)(2,1)S(1)}, u32[]{:S(2)}, u32[]{:S(2)}) collective-permute-start(bf16[40,2048]{1,0:T(8,128)(2,1)S(1)} %get-tuple-element.49), channel_id=1, source_target_pairs={{0,8},{4,12},{8,0},{12,4},{16,24},{20,28},{24,16},{28,20},{1,9},{5... | collective-permute-start | bytes 491528 | tf_op jit(solution)/shard_map/ppermute | solution.py:27
  (28 other events, 308.7 us)

commit v2 on v1

--- a/solution.py
+++ b/solution.py
@@ -174,7 +174,7 @@
     gate_ref, up_ref, down_ref = refs[count : count + 3]
     outputs = refs[count + 3 : -1]
     hidden_ref = refs[-1]
-    rows, width = inputs[0].shape
+    _, width = inputs[0].shape
     tile, wide = 128, min(512, width)
     order = list(range(0, count, 2)) + list(range(1, count, 2))
 
@@ -197,9 +197,8 @@
             first += ref.shape[0]
         return carry
 
-    short = count * rows <= 512
-    lax.fori_loop(0, gate_ref.shape[1] // tile, hidden_step, 0, unroll=short)
-    lax.fori_loop(0, width // wide, down_step, 0, unroll=short)
+    lax.fori_loop(0, gate_ref.shape[1] // tile, hidden_step, 0, unroll=True)
+    lax.fori_loop(0, width // wide, down_step, 0, unroll=True)
 
 
 def expert(blocks, gate, up, down):
@@ -306,6 +305,8 @@
     smem = pl.BlockSpec(memory_space=pltpu.SMEM)
     scratch = 4 * total_keys * value_size + 16 * rows * (total_keys + 128)
     room = scratch + 2 * blocks[0].size * len(blocks) + attention_margin
+    scratch = 4 * total_keys * value_size + 16 * rows * (total_keys + 128)
+    room = scratch + 2 * blocks[0].size * len(blocks) + attention_margin
     return pl.pallas_call(
         functools.partial(attention_kernel, heads, head_size, value_size, rows, len(blocks)),
         out_shape=jax.ShapeDtypeStruct((queries, heads * value_size), jnp.bfloat16),

time: 196 us -> 196 us (level)
  transfers between devices with their start and end apart: 46 -> 46, of which waited for: 18 -> 18; matrix products, arithmetic and copies ran while one was open for 1% -> 1% of each run, Pallas kernels for 17% -> 16%
where the time goes in v2:
time: 196 us
  waiting for transfers between devices  80.7 us (41%)
  starting transfers between devices  69.7 us (36%)
  Pallas kernels  34.9 us (18%)
  local copies, waits for them, and re-layouts  8.02 us (4%)
    ppermute x46, waiting for transfers between devices, swap(): return lax.ppermute(array, axis, [(i, i ^ mask) for i in range(size)])  80.7 us
    ppermute x46, starting transfers between devices, swap(): return lax.ppermute(array, axis, [(i, i ^ mask) for i in range(size)])  69.7 us
    pallas_call x3, Pallas kernels, expert(): pl.pallas_call(functools.partial(expert_kernel, count), out_shape=shapes,...  17.9 us
    pallas_call x2, Pallas kernels, attention(): pl.pallas_call(functools.partial(attention_kernel, heads, head_size, valu...  11.5 us
    unnamed x33, local copies, waits for them, and re-layouts  6.6 us
  transfers between devices with their start and end apart: 46, of which 18 were waited for; matrix products, arithmetic and copies ran while one was open for 1% of the time, Pallas kernels for 16%

profile of v2, /device:TPU:0, one launch (start us, length us, event | category | flops | bytes accessed | tf_op | source)
XLA Modules:
  0.0 195.5 jit_solution(1591122387179597253)
XLA Ops:
  4.4 5.1 %collective-permute-start.37 = (bf16[40,2048]{1,0:T(8,128)(2,1)S(1)}, bf16[40,2048]{1,0:T(8,128)(2,1)S(1)}, u32[]{:S(2)}, u32[]{:S(2)}) collective-permute-start(bf16[40,2048]{1,0:T(8,128)(2,1)S(1)} %get-tuple-element.41), channel_id=1, source_target_pairs={{0,24},{4,28},{8,16},{12,20},{16,8},{20,12},{24,0},{28,4},{1,25},{... | collective-permute-start | bytes 491528 | tf_op jit(solution)/shard_map/ppermute | solution.py:27
  11.5 1.9 collective-permute-start.29
  13.4 1.7 collective-permute-start.17
  17.1 11.3 %collective-permute-start.18 = (bf16[40,2048]{1,0:T(8,128)(2,1)S(1)}, bf16[40,2048]{1,0:T(8,128)(2,1)S(1)}, u32[]{:S(2)}, u32[]{:S(2)}) collective-permute-start(bf16[40,2048]{1,0:T(8,128)(2,1)S(1)} %get-tuple-element.31), channel_id=1, source_target_pairs={{0,8},{4,12},{8,0},{12,4},{16,24},{20,28},{24,16},{28,20},{1,9},{5... | collective-permute-start | bytes 491528 | tf_op jit(solution)/shard_map/ppermute | solution.py:27
  28.4 6.5 %collective-permute-done.28 = bf16[40,2048]{1,0:T(8,128)(2,1)S(1)} collective-permute-done((bf16[40,2048]{1,0:T(8,128)(2,1)S(1)}, bf16[40,2048]{1,0:T(8,128)(2,1)S(1)}, u32[]{:S(2)}, u32[]{:S(2)}) %collective-permute-start.28) | collective-permute-done | bytes 163872 | tf_op jit(solution)/shard_map/ppermute | solution.py:27
  35.8 2.3 %collective-permute-start.3 = (bf16[512,384]{1,0:T(8,128)(2,1)S(1)}, bf16[512,384]{1,0:T(8,128)(2,1)S(1)}, u32[]{:S(2)}, u32[]{:S(2)}) collective-permute-start(bf16[512,384]{1,0:T(8,128)(2,1)S(1)} %get-tuple-element.26), channel_id=1, source_target_pairs={{0,8},{4,12},{8,0},{12,4},{16,24},{20,28},{24,16},{28,20},{1,9},{5... | collective-permute-start | bytes 1179656 | tf_op jit(solution)/shard_map/ppermute | solution.py:27
  40.9 8.1 %collective-permute-done.40.refs_2_ = bf16[80,2048]{1,0:T(8,128)(2,1)S(1)} collective-permute-done((bf16[80,2048]{1,0:T(8,128)(2,1)S(1)}, bf16[80,2048]{1,0:T(8,128)(2,1)S(1)}, u32[]{:S(2)}, u32[]{:S(2)}) %collective-permute-start.40) | collective-permute-done | bytes 327712 | tf_op jit(solution)/shard_map/ppermute | solution.py:27
  52.1 2.8 %collective-permute-done.31.refs_2_ = bf16[80,2048]{1,0:T(8,128)(2,1)S(1)} collective-permute-done((bf16[80,2048]{1,0:T(8,128)(2,1)S(1)}, bf16[80,2048]{1,0:T(8,128)(2,1)S(1)}, u32[]{:S(2)}, u32[]{:S(2)}) %collective-permute-start.31) | collective-permute-done | bytes 327712 | tf_op jit(solution)/shard_map/ppermute | solution.py:27
  54.9 2.0 %copy-done.1 = bf16[1,2048,896]{2,1,0:T(8,128)(2,1)S(1)} copy-done((bf16[1,2048,896]{2,1,0:T(8,128)(2,1)S(1)}, bf16[1,2048,896]{2,1,0:T(8,128)(2,1)}, u32[]{:S(2)}) %copy-start.1) | copy-done | bytes 3670040
  56.9 2.0 %copy-done.3 = bf16[1,896,2048]{2,1,0:T(8,128)(2,1)S(1)} copy-done((bf16[1,896,2048]{2,1,0:T(8,128)(2,1)S(1)}, bf16[1,896,2048]{2,1,0:T(8,128)(2,1)}, u32[]{:S(2)}) %copy-start.3) | copy-done | bytes 3670040
  59.0 4.5 %shard_map.144 = (bf16[80,2048]{1,0:T(8,128)(2,1)S(1)}, bf16[80,2048]{1,0:T(8,128)(2,1)S(1)}, bf16[160,2048]{1,0:T(8,128)(2,1)S(1)}) custom-call(bf16[80,2048]{1,0:T(8,128)(2,1)S(1)} %constant_dynamic-update-slice_fusion.6.refs_0_, bf16[80,2048]{1,0:T(8,128)(2,1)S(1)} %collective-permute-done.39.refs_1_, ...), custom_call_target="tpu_custom_call" | custom-call | flops 3523215360 | bytes 13631488 | tf_op jit(solution)/shard_map/pallas_call | solution.py:211
  63.5 6.4 %collective-permute-done.1.refs_2_ = bf16[512,256]{1,0:T(8,128)(2,1)S(1)} collective-permute-done((bf16[512,256]{1,0:T(8,128)(2,1)S(1)}, bf16[512,256]{1,0:T(8,128)(2,1)S(1)}, u32[]{:S(2)}, u32[]{:S(2)}) %collective-permute-start.1) | collective-permute-done | bytes 262176 | tf_op jit(solution)/shard_map/ppermute | solution.py:27
  72.0 3.5 %collective-permute-done.5.refs_6_ = bf16[512,256]{1,0:T(8,128)(2,1)S(1)} collective-permute-done((bf16[512,256]{1,0:T(8,128)(2,1)S(1)}, bf16[512,256]{1,0:T(8,128)(2,1)S(1)}, u32[]{:S(2)}, u32[]{:S(2)}) %collective-permute-start.5) | collective-permute-done | bytes 262176 | tf_op jit(solution)/shard_map/ppermute | solution.py:27
  77.5 4.5 %shard_map.143 = (bf16[80,2048]{1,0:T(8,128)(2,1)S(1)}, bf16[80,2048]{1,0:T(8,128)(2,1)S(1)}, bf16[160,2048]{1,0:T(8,128)(2,1)S(1)}) custom-call(bf16[80,2048]{1,0:T(8,128)(2,1)S(1)} %constant_dynamic-update-slice_fusion.4.refs_0_, bf16[80,2048]{1,0:T(8,128)(2,1)S(1)} %collective-permute-done.30.refs_1_, ...), custom_call_target="tpu_custom_call" | custom-call | flops 3523215360 | bytes 13631488 | tf_op jit(solution)/shard_map/pallas_call | solution.py:211
  84.7 5.6 %collective-permute-done.4.refs_5_ = bf16[512,256]{1,0:T(8,128)(2,1)S(1)} collective-permute-done((bf16[512,256]{1,0:T(8,128)(2,1)S(1)}, bf16[512,256]{1,0:T(8,128)(2,1)S(1)}, u32[]{:S(2)}, u32[]{:S(2)}) %collective-permute-start.4) | collective-permute-done | bytes 262176 | tf_op jit(solution)/shard_map/ppermute | solution.py:27
  90.8 4.2 %collective-permute-done.6.refs_7_ = bf16[512,256]{1,0:T(8,128)(2,1)S(1)} collective-permute-done((bf16[512,256]{1,0:T(8,128)(2,1)S(1)}, bf16[512,256]{1,0:T(8,128)(2,1)S(1)}, u32[]{:S(2)}, u32[]{:S(2)}) %collective-permute-start.6) | collective-permute-done | bytes 262176 | tf_op jit(solution)/shard_map/ppermute | solution.py:27
  95.0 5.8 %shard_map.141 = bf16[512,128]{1,0:T(8,128)(2,1)S(1)} custom-call(s32[3]{0:T(128)S(1)} %pad_add_fusion.place_ref, f32[2]{0:T(128)S(1)} %copy-done.12, f32[1,128]{1,0:T(1,128)S(1)} %bitcast.25, bf16[512,128]{1,0:T(8,128)(2,1)S(1)} %slice.89.q_ref, bf16[512,256]{1,0:T(8,128)(2,1)S(1)} %get-tuple-element.25.refs_0_, ...), custom_call_target="tpu_custom_call" | custom-call | flops 3221225472 | bytes 2097152 | tf_op jit(solution)/shard_map/pallas_call | solution.py:310
  101.0 5.7 %shard_map.140 = bf16[512,128]{1,0:T(8,128)(2,1)S(1)} custom-call(s32[3]{0:T(128)S(1)} %pad_add_fusion.place_ref, f32[2]{0:T(128)S(1)} %copy-done.12, f32[1,128]{1,0:T(1,128)S(1)} %bitcast.26, bf16[512,128]{1,0:T(8,128)(2,1)S(1)} %get-tuple-element.24.q_ref, bf16[512,256]{1,0:T(8,128)(2,1)S(1)} %get-tuple-element.25.refs_0_, ...), custom_call_target="tpu_custom_call" | custom-call | flops 3221225472 | bytes 2097152 | tf_op jit(solution)/shard_map/pallas_call | solution.py:310
  109.3 8.8 %shard_map.142 = (bf16[160,2048]{1,0:T(8,128)(2,1)S(1)}, bf16[160,2048]{1,0:T(8,128)(2,1)S(1)}, bf16[320,2048]{1,0:T(8,128)(2,1)S(1)}) custom-call(bf16[160,2048]{1,0:T(8,128)(2,1)S(1)} %constant_dynamic-update-slice_fusion.refs_0_, bf16[160,2048]{1,0:T(8,128)(2,1)S(1)} %collective-permute-done.20.refs_1_, ...), custom_call_target="tpu_custom_call" | custom-call | flops 7046430720 | bytes 16252928 | tf_op jit(solution)/shard_map/pallas_call | solution.py:211
  118.3 9.9 %collective-permute-done.43 = bf16[80,2048]{1,0:T(8,128)(2,1)S(1)} collective-permute-done((bf16[80,2048]{1,0:T(8,128)(2,1)S(1)}, bf16[80,2048]{1,0:T(8,128)(2,1)S(1)}, u32[]{:S(2)}, u32[]{:S(2)}) %collective-permute-start.43) | collective-permute-done | bytes 327712 | tf_op jit(solution)/shard_map/ppermute | solution.py:27
  130.4 7.0 %collective-permute-done.34 = bf16[80,2048]{1,0:T(8,128)(2,1)S(1)} collective-permute-done((bf16[80,2048]{1,0:T(8,128)(2,1)S(1)}, bf16[80,2048]{1,0:T(8,128)(2,1)S(1)}, u32[]{:S(2)}, u32[]{:S(2)}) %collective-permute-start.34) | collective-permute-done | bytes 327712 | tf_op jit(solution)/shard_map/ppermute | solution.py:27
  139.4 15.6 %collective-permute-done.24 = bf16[160,2048]{1,0:T(8,128)(2,1)S(1)} collective-permute-done((bf16[160,2048]{1,0:T(8,128)(2,1)S(1)}, bf16[160,2048]{1,0:T(8,128)(2,1)S(1)}, u32[]{:S(2)}, u32[]{:S(2)}) %collective-permute-start.24) | collective-permute-done | bytes 655392 | tf_op jit(solution)/shard_map/ppermute | solution.py:27
  157.5 1.7 collective-permute-start.44
  159.2 2.1 %collective-permute-start.45 = (bf16[40,2048]{1,0:T(8,128)(2,1)S(1)}, bf16[40,2048]{1,0:T(8,128)(2,1)S(1)}, u32[]{:S(2)}, u32[]{:S(2)}) collective-permute-start(bf16[40,2048]{1,0:T(8,128)(2,1)S(1)} %get-tuple-element.52), channel_id=1, source_target_pairs={{0,28},{4,24},{8,20},{12,16},{16,12},{20,8},{24,4},{28,0},{1,29},{... | collective-permute-start | bytes 491528 | tf_op jit(solution)/shard_map/ppermute | solution.py:27
  162.1 3.2 %collective-permute-start.36 = (bf16[40,2048]{1,0:T(8,128)(2,1)S(1)}, bf16[40,2048]{1,0:T(8,128)(2,1)S(1)}, u32[]{:S(2)}, u32[]{:S(2)}) collective-permute-start(bf16[40,2048]{1,0:T(8,128)(2,1)S(1)} %get-tuple-element.54), channel_id=1, source_target_pairs={{0,20},{4,16},{8,28},{12,24},{16,4},{20,0},{24,12},{28,8},{1,21},{... | collective-permute-start | bytes 491528 | tf_op jit(solution)/shard_map/ppermute | solution.py:27
  166.5 13.5 %collective-permute-start.26 = (bf16[40,2048]{1,0:T(8,128)(2,1)S(1)}, bf16[40,2048]{1,0:T(8,128)(2,1)S(1)}, u32[]{:S(2)}, u32[]{:S(2)}) collective-permute-start(bf16[40,2048]{1,0:T(8,128)(2,1)S(1)} %get-tuple-element.49), channel_id=1, source_target_pairs={{0,8},{4,12},{8,0},{12,4},{16,24},{20,28},{24,16},{28,20},{1,9},{5... | collective-permute-start | bytes 491528 | tf_op jit(solution)/shard_map/ppermute | solution.py:27
  180.0 4.4 %collective-permute-start.27 = (bf16[40,2048]{1,0:T(8,128)(2,1)S(1)}, bf16[40,2048]{1,0:T(8,128)(2,1)S(1)}, u32[]{:S(2)}, u32[]{:S(2)}) collective-permute-start(bf16[40,2048]{1,0:T(8,128)(2,1)S(1)} %get-tuple-element.48), channel_id=1, source_target_pairs={{0,12},{4,8},{8,4},{12,0},{16,28},{20,24},{24,20},{28,16},{1,13},{... | collective-permute-start | bytes 491528 | tf_op jit(solution)/shard_map/ppermute | solution.py:27
  184.4 2.1 %mixer.1 = bf16[128,2048]{1,0:T(8,128)(2,1)} custom-call(s32[3]{0:T(128)S(1)} %pad_add_fusion.place_ref, bf16[128,256]{1,0:T(8,128)(2,1)S(1)} %get-tuple-element.57.refs_0_, bf16[128,256]{1,0:T(8,128)(2,1)S(1)} %collective-permute-done.8.refs_1_, bf16[128,256]{1,0:T(8,128)(2,1)S(1)} %collective-permute-done.9.refs_2_, ...), custom_call_target="tpu_custom_call" | custom-call | flops 536870912 | bytes 4194304 | tf_op jit(solution)/shard_map/mixer/pallas_call | solution.py:344
  186.5 3.0 %collective-permute-done.36.refs_5_ = bf16[40,2048]{1,0:T(8,128)(2,1)S(1)} collective-permute-done((bf16[40,2048]{1,0:T(8,128)(2,1)S(1)}, bf16[40,2048]{1,0:T(8,128)(2,1)S(1)}, u32[]{:S(2)}, u32[]{:S(2)}) %collective-permute-start.36) | collective-permute-done | bytes 163872 | tf_op jit(solution)/shard_map/ppermute | solution.py:27
  189.5 2.0 collective-permute-done.26.refs_2_
  191.5 2.5 %collective-permute-done.27.refs_3_ = bf16[40,2048]{1,0:T(8,128)(2,1)S(1)} collective-permute-done((bf16[40,2048]{1,0:T(8,128)(2,1)S(1)}, bf16[40,2048]{1,0:T(8,128)(2,1)S(1)}, u32[]{:S(2)}, u32[]{:S(2)}) %collective-permute-start.27) | collective-permute-done | bytes 163872 | tf_op jit(solution)/shard_map/ppermute | solution.py:27
  194.0 1.6 combine.1
  (120 shorter events, 32.9 us)
Async XLA Ops:
  9.5 26.2 %collective-permute-start.38 = (bf16[40,2048]{1,0:T(8,128)(2,1)S(1)}, bf16[40,2048]{1,0:T(8,128)(2,1)S(1)}, u32[]{:S(2)}, u32[]{:S(2)}) collective-permute-start(bf16[40,2048]{1,0:T(8,128)(2,1)S(1)} %get-tuple-element.42), channel_id=1, source_target_pairs={{0,28},{4,24},{8,20},{12,16},{16,12},{20,8},{24,4},{28,0},{1,29},{... | collective-permute-start | bytes 491528 | tf_op jit(solution)/shard_map/ppermute | solution.py:27
  10.7 24.3 %collective-permute-start.28 = (bf16[40,2048]{1,0:T(8,128)(2,1)S(1)}, bf16[40,2048]{1,0:T(8,128)(2,1)S(1)}, u32[]{:S(2)}, u32[]{:S(2)}) collective-permute-start(bf16[40,2048]{1,0:T(8,128)(2,1)S(1)} %get-tuple-element.36), channel_id=1, source_target_pairs={{0,16},{4,20},{8,24},{12,28},{16,0},{20,4},{24,8},{28,12},{1,17},{... | collective-permute-start | bytes 491528 | tf_op jit(solution)/shard_map/ppermute | solution.py:27
  11.5 27.0 %collective-permute-start.29 = (bf16[40,2048]{1,0:T(8,128)(2,1)S(1)}, bf16[40,2048]{1,0:T(8,128)(2,1)S(1)}, u32[]{:S(2)}, u32[]{:S(2)}) collective-permute-start(bf16[40,2048]{1,0:T(8,128)(2,1)S(1)} %get-tuple-element.37), channel_id=1, source_target_pairs={{0,20},{4,16},{8,28},{12,24},{16,4},{20,0},{24,12},{28,8},{1,21},{... | collective-permute-start | bytes 491528 | tf_op jit(solution)/shard_map/ppermute | solution.py:27
  13.4 26.6 %collective-permute-start.17 = (bf16[40,2048]{1,0:T(8,128)(2,1)S(1)}, bf16[40,2048]{1,0:T(8,128)(2,1)S(1)}, u32[]{:S(2)}, u32[]{:S(2)}) collective-permute-start(bf16[40,2048]{1,0:T(8,128)(2,1)S(1)} %get-tuple-element.30), channel_id=1, source_target_pairs={{0,4},{4,0},{8,12},{12,8},{16,20},{20,16},{24,28},{28,24},{1,5},{5... | collective-permute-start | bytes 491528 | tf_op jit(solution)/shard_map/ppermute | solution.py:27
  17.1 23.0 %collective-permute-start.18 = (bf16[40,2048]{1,0:T(8,128)(2,1)S(1)}, bf16[40,2048]{1,0:T(8,128)(2,1)S(1)}, u32[]{:S(2)}, u32[]{:S(2)}) collective-permute-start(bf16[40,2048]{1,0:T(8,128)(2,1)S(1)} %get-tuple-element.31), channel_id=1, source_target_pairs={{0,8},{4,12},{8,0},{12,4},{16,24},{20,28},{24,16},{28,20},{1,9},{5... | collective-permute-start | bytes 491528 | tf_op jit(solution)/shard_map/ppermute | solution.py:27
  35.8 14.7 %collective-permute-start.3 = (bf16[512,384]{1,0:T(8,128)(2,1)S(1)}, bf16[512,384]{1,0:T(8,128)(2,1)S(1)}, u32[]{:S(2)}, u32[]{:S(2)}) collective-permute-start(bf16[512,384]{1,0:T(8,128)(2,1)S(1)} %get-tuple-element.26), channel_id=1, source_target_pairs={{0,8},{4,12},{8,0},{12,4},{16,24},{20,28},{24,16},{28,20},{1,9},{5... | collective-permute-start | bytes 1179656 | tf_op jit(solution)/shard_map/ppermute | solution.py:27
  40.1 14.7 %collective-permute-start.31 = (bf16[80,2048]{1,0:T(8,128)(2,1)S(1)}, bf16[80,2048]{1,0:T(8,128)(2,1)S(1)}, u32[]{:S(2)}, u32[]{:S(2)}) collective-permute-start(bf16[80,2048]{1,0:T(8,128)(2,1)S(1)} %constant_dynamic-update-slice_fusion.4.refs_0_), channel_id=1, source_target_pairs={{0,2},{1,3},{2,0},{3,1},{4,6},{5,7},{6,4},{7,5},{8,10},{9,11},{10,... | collective-permute-start | bytes 983048 | tf_op jit(solution)/shard_map/ppermute | solution.py:27
  49.1 20.8 %collective-permute-start.1 = (bf16[512,256]{1,0:T(8,128)(2,1)S(1)}, bf16[512,256]{1,0:T(8,128)(2,1)S(1)}, u32[]{:S(2)}, u32[]{:S(2)}) collective-permute-start(bf16[512,256]{1,0:T(8,128)(2,1)S(1)} %get-tuple-element.25.refs_0_), channel_id=1, source_target_pairs={{0,16},{4,20},{8,24},{12,28},{16,0},{20,4},{24,8},{28,12},{1,17},{... | collective-permute-start | bytes 786440 | tf_op jit(solution)/shard_map/ppermute | solution.py:27
  50.4 20.0 %collective-permute-start.30 = (bf16[80,2048]{1,0:T(8,128)(2,1)S(1)}, bf16[80,2048]{1,0:T(8,128)(2,1)S(1)}, u32[]{:S(2)}, u32[]{:S(2)}) collective-permute-start(bf16[80,2048]{1,0:T(8,128)(2,1)S(1)} %constant_dynamic-update-slice_fusion.4.refs_0_), channel_id=1, source_target_pairs={{0,1},{1,0},{2,3},{3,2},{4,5},{5,4},{6,7},{7,6},{8,9},{9,8},{10,11... | collective-permute-start | bytes 983048 | tf_op jit(solution)/shard_map/ppermute | solution.py:27
  50.5 39.8 %collective-permute-start.21 = (bf16[160,2048]{1,0:T(8,128)(2,1)S(1)}, bf16[160,2048]{1,0:T(8,128)(2,1)S(1)}, u32[]{:S(2)}, u32[]{:S(2)}) collective-permute-start(bf16[160,2048]{1,0:T(8,128)(2,1)S(1)} %constant_dynamic-update-slice_fusion.refs_0_), channel_id=1, source_target_pairs={{0,2},{1,3},{2,0},{3,1},{4,6},{5,7},{6,4},{7,5},{8,10},{9,11},{10,... | collective-permute-start | bytes 1966088 | tf_op jit(solution)/shard_map/ppermute | solution.py:27
  54.9 20.6 %collective-permute-start.5 = (bf16[512,256]{1,0:T(8,128)(2,1)S(1)}, bf16[512,256]{1,0:T(8,128)(2,1)S(1)}, u32[]{:S(2)}, u32[]{:S(2)}) collective-permute-start(bf16[512,256]{1,0:T(8,128)(2,1)S(1)} %slice.88.refs_4_), channel_id=1, source_target_pairs={{0,16},{4,20},{8,24},{12,28},{16,0},{20,4},{24,8},{28,12},{1,17},{... | collective-permute-start | bytes 786440 | tf_op jit(solution)/shard_map/ppermute | solution.py:27
  54.9 21.1 %collective-permute-start.32 = (bf16[80,2048]{1,0:T(8,128)(2,1)S(1)}, bf16[80,2048]{1,0:T(8,128)(2,1)S(1)}, u32[]{:S(2)}, u32[]{:S(2)}) collective-permute-start(bf16[80,2048]{1,0:T(8,128)(2,1)S(1)} %collective-permute-done.31.refs_2_), channel_id=1, source_target_pairs={{0,1},{1,0},{2,3},{3,2},{4,5},{5,4},{6,7},{7,6},{8,9},{9,8},{10,11... | collective-permute-start | bytes 983048 | tf_op jit(solution)/shard_map/ppermute | solution.py:27
  70.4 14.3 %collective-permute-start.2 = (bf16[512,256]{1,0:T(8,128)(2,1)S(1)}, bf16[512,256]{1,0:T(8,128)(2,1)S(1)}, u32[]{:S(2)}, u32[]{:S(2)}) collective-permute-start(bf16[512,256]{1,0:T(8,128)(2,1)S(1)} %collective-permute-done.1.refs_2_), channel_id=1, source_target_pairs={{0,4},{4,0},{8,12},{12,8},{16,20},{20,16},{24,28},{28,24},{1,5},{5... | collective-permute-start | bytes 786440 | tf_op jit(solution)/shard_map/ppermute | solution.py:27
  75.5 14.8 %collective-permute-start.4 = (bf16[512,256]{1,0:T(8,128)(2,1)S(1)}, bf16[512,256]{1,0:T(8,128)(2,1)S(1)}, u32[]{:S(2)}, u32[]{:S(2)}) collective-permute-start(bf16[512,256]{1,0:T(8,128)(2,1)S(1)} %slice.88.refs_4_), channel_id=1, source_target_pairs={{0,4},{4,0},{8,12},{12,8},{16,20},{20,16},{24,28},{28,24},{1,5},{5... | collective-permute-start | bytes 786440 | tf_op jit(solution)/shard_map/ppermute | solution.py:27
  76.0 19.0 %collective-permute-start.6 = (bf16[512,256]{1,0:T(8,128)(2,1)S(1)}, bf16[512,256]{1,0:T(8,128)(2,1)S(1)}, u32[]{:S(2)}, u32[]{:S(2)}) collective-permute-start(bf16[512,256]{1,0:T(8,128)(2,1)S(1)} %collective-permute-done.5.refs_6_), channel_id=1, source_target_pairs={{0,4},{4,0},{8,12},{12,8},{16,20},{20,16},{24,28},{28,24},{1,5},{5... | collective-permute-start | bytes 786440 | tf_op jit(solution)/shard_map/ppermute | solution.py:27
  82.1 47.7 %collective-permute-start.13 = (bf16[128,2048]{1,0:T(8,128)(2,1)S(1)}, bf16[128,2048]{1,0:T(8,128)(2,1)S(1)}, u32[]{:S(2)}, u32[]{:S(2)}) collective-permute-start(bf16[128,2048]{1,0:T(8,128)(2,1)S(1)} %get-tuple-element.47.refs_4_), channel_id=1, source_target_pairs={{0,2},{1,3},{2,0},{3,1},{4,6},{5,7},{6,4},{7,5},{8,10},{9,11},{10,... | collective-permute-start | bytes 1572872 | tf_op jit(solution)/shard_map/ppermute | solution.py:27
  84.7 23.7 %collective-permute-start.20 = (bf16[160,2048]{1,0:T(8,128)(2,1)S(1)}, bf16[160,2048]{1,0:T(8,128)(2,1)S(1)}, u32[]{:S(2)}, u32[]{:S(2)}) collective-permute-start(bf16[160,2048]{1,0:T(8,128)(2,1)S(1)} %constant_dynamic-update-slice_fusion.refs_0_), channel_id=1, source_target_pairs={{0,1},{1,0},{2,3},{3,2},{4,5},{5,4},{6,7},{7,6},{8,9},{9,8},{10,11... | collective-permute-start | bytes 1966088 | tf_op jit(solution)/shard_map/ppermute | solution.py:27
  90.3 16.4 %collective-permute-start.42 = (bf16[160,2048]{1,0:T(8,128)(2,1)S(1)}, bf16[160,2048]{1,0:T(8,128)(2,1)S(1)}, u32[]{:S(2)}, u32[]{:S(2)}) collective-permute-start(bf16[160,2048]{1,0:T(8,128)(2,1)S(1)} %get-tuple-element.44), channel_id=1, source_target_pairs={{0,1},{1,0},{2,3},{3,2},{4,5},{5,4},{6,7},{7,6},{8,9},{9,8},{10,11... | collective-permute-start | bytes 1966088 | tf_op jit(solution)/shard_map/ppermute | solution.py:27
  90.3 18.4 %collective-permute-start.22 = (bf16[160,2048]{1,0:T(8,128)(2,1)S(1)}, bf16[160,2048]{1,0:T(8,128)(2,1)S(1)}, u32[]{:S(2)}, u32[]{:S(2)}) collective-permute-start(bf16[160,2048]{1,0:T(8,128)(2,1)S(1)} %collective-permute-done.21.refs_2_), channel_id=1, source_target_pairs={{0,1},{1,0},{2,3},{3,2},{4,5},{5,4},{6,7},{7,6},{8,9},{9,8},{10,11... | collective-permute-start | bytes 1966088 | tf_op jit(solution)/shard_map/ppermute | solution.py:27
  106.6 49.4 %collective-permute-start.11 = (bf16[128,2048]{1,0:T(8,128)(2,1)S(1)}, bf16[128,2048]{1,0:T(8,128)(2,1)S(1)}, u32[]{:S(2)}, u32[]{:S(2)}) collective-permute-start(bf16[128,2048]{1,0:T(8,128)(2,1)S(1)} %get-tuple-element.47.refs_4_), channel_id=1, source_target_pairs={{0,1},{1,0},{2,3},{3,2},{4,5},{5,4},{6,7},{7,6},{8,9},{9,8},{10,11... | collective-permute-start | bytes 1572872 | tf_op jit(solution)/shard_map/ppermute | solution.py:27
  106.8 23.1 %collective-permute-start.14 = (bf16[128,2048]{1,0:T(8,128)(2,1)S(1)}, bf16[128,2048]{1,0:T(8,128)(2,1)S(1)}, u32[]{:S(2)}, u32[]{:S(2)}) collective-permute-start(bf16[128,2048]{1,0:T(8,128)(2,1)S(1)} %get-tuple-element.46.refs_5_), channel_id=1, source_target_pairs={{0,2},{1,3},{2,0},{3,1},{4,6},{5,7},{6,4},{7,5},{8,10},{9,11},{10,... | collective-permute-start | bytes 1572872 | tf_op jit(solution)/shard_map/ppermute | solution.py:27
  108.7 19.5 %collective-permute-start.43 = (bf16[80,2048]{1,0:T(8,128)(2,1)S(1)}, bf16[80,2048]{1,0:T(8,128)(2,1)S(1)}, u32[]{:S(2)}, u32[]{:S(2)}) collective-permute-start(bf16[80,2048]{1,0:T(8,128)(2,1)S(1)} %add_convert_fusion.4), channel_id=1, source_target_pairs={{0,2},{1,3},{2,0},{3,1},{4,6},{5,7},{6,4},{7,5},{8,10},{9,11},{10,... | collective-permute-start | bytes 983048 | tf_op jit(solution)/shard_map/ppermute | solution.py:27
  118.1 19.5 %collective-permute-start.23 = (bf16[320,2048]{1,0:T(8,128)(2,1)S(1)}, bf16[320,2048]{1,0:T(8,128)(2,1)S(1)}, u32[]{:S(2)}, u32[]{:S(2)}) collective-permute-start(bf16[320,2048]{1,0:T(8,128)(2,1)S(1)} %get-tuple-element.34), channel_id=1, source_target_pairs={{0,1},{1,0},{2,3},{3,2},{4,5},{5,4},{6,7},{7,6},{8,9},{9,8},{10,11... | collective-permute-start | bytes 3932168 | tf_op jit(solution)/shard_map/ppermute | solution.py:27
  129.8 27.2 %collective-permute-start.12 = (bf16[128,2048]{1,0:T(8,128)(2,1)S(1)}, bf16[128,2048]{1,0:T(8,128)(2,1)S(1)}, u32[]{:S(2)}, u32[]{:S(2)}) collective-permute-start(bf16[128,2048]{1,0:T(8,128)(2,1)S(1)} %get-tuple-element.46.refs_5_), channel_id=1, source_target_pairs={{0,1},{1,0},{2,3},{3,2},{4,5},{5,4},{6,7},{7,6},{8,9},{9,8},{10,11... | collective-permute-start | bytes 1572872 | tf_op jit(solution)/shard_map/ppermute | solution.py:27
  129.9 27.6 %collective-permute-start.15 = (bf16[128,2048]{1,0:T(8,128)(2,1)S(1)}, bf16[128,2048]{1,0:T(8,128)(2,1)S(1)}, u32[]{:S(2)}, u32[]{:S(2)}) collective-permute-start(bf16[128,2048]{1,0:T(8,128)(2,1)S(1)} %collective-permute-done.13.refs_8_), channel_id=1, source_target_pairs={{0,1},{1,0},{2,3},{3,2},{4,5},{5,4},{6,7},{7,6},{8,9},{9,8},{10,11... | collective-permute-start | bytes 1572872 | tf_op jit(solution)/shard_map/ppermute | solution.py:27
  137.4 21.8 %collective-permute-start.16 = (bf16[128,2048]{1,0:T(8,128)(2,1)S(1)}, bf16[128,2048]{1,0:T(8,128)(2,1)S(1)}, u32[]{:S(2)}, u32[]{:S(2)}) collective-permute-start(bf16[128,2048]{1,0:T(8,128)(2,1)S(1)} %collective-permute-done.14.refs_9_), channel_id=1, source_target_pairs={{0,1},{1,0},{2,3},{3,2},{4,5},{5,4},{6,7},{7,6},{8,9},{9,8},{10,11... | collective-permute-start | bytes 1572872 | tf_op jit(solution)/shard_map/ppermute | solution.py:27
  137.8 17.2 %collective-permute-start.24 = (bf16[160,2048]{1,0:T(8,128)(2,1)S(1)}, bf16[160,2048]{1,0:T(8,128)(2,1)S(1)}, u32[]{:S(2)}, u32[]{:S(2)}) collective-permute-start(bf16[160,2048]{1,0:T(8,128)(2,1)S(1)} %add_convert_fusion.1), channel_id=1, source_target_pairs={{0,2},{1,3},{2,0},{3,1},{4,6},{5,7},{6,4},{7,5},{8,10},{9,11},{10,... | collective-permute-start | bytes 1966088 | tf_op jit(solution)/shard_map/ppermute | solution.py:27
  159.2 20.7 %collective-permute-start.45 = (bf16[40,2048]{1,0:T(8,128)(2,1)S(1)}, bf16[40,2048]{1,0:T(8,128)(2,1)S(1)}, u32[]{:S(2)}, u32[]{:S(2)}) collective-permute-start(bf16[40,2048]{1,0:T(8,128)(2,1)S(1)} %get-tuple-element.52), channel_id=1, source_target_pairs={{0,28},{4,24},{8,20},{12,16},{16,12},{20,8},{24,4},{28,0},{1,29},{... | collective-permute-start | bytes 491528 | tf_op jit(solution)/shard_map/ppermute | solution.py:27
  161.4 25.1 %collective-permute-start.35 = (bf16[40,2048]{1,0:T(8,128)(2,1)S(1)}, bf16[40,2048]{1,0:T(8,128)(2,1)S(1)}, u32[]{:S(2)}, u32[]{:S(2)}) collective-permute-start(bf16[40,2048]{1,0:T(8,128)(2,1)S(1)} %get-tuple-element.55), channel_id=1, source_target_pairs={{0,16},{4,20},{8,24},{12,28},{16,0},{20,4},{24,8},{28,12},{1,17},{... | collective-permute-start | bytes 491528 | tf_op jit(solution)/shard_map/ppermute | solution.py:27
  162.1 27.4 %collective-permute-start.36 = (bf16[40,2048]{1,0:T(8,128)(2,1)S(1)}, bf16[40,2048]{1,0:T(8,128)(2,1)S(1)}, u32[]{:S(2)}, u32[]{:S(2)}) collective-permute-start(bf16[40,2048]{1,0:T(8,128)(2,1)S(1)} %get-tuple-element.54), channel_id=1, source_target_pairs={{0,20},{4,16},{8,28},{12,24},{16,4},{20,0},{24,12},{28,8},{1,21},{... | collective-permute-start | bytes 491528 | tf_op jit(solution)/shard_map/ppermute | solution.py:27
  165.3 24.2 %collective-permute-start.25 = (bf16[40,2048]{1,0:T(8,128)(2,1)S(1)}, bf16[40,2048]{1,0:T(8,128)(2,1)S(1)}, u32[]{:S(2)}, u32[]{:S(2)}) collective-permute-start(bf16[40,2048]{1,0:T(8,128)(2,1)S(1)} %get-tuple-element.50), channel_id=1, source_target_pairs={{0,4},{4,0},{8,12},{12,8},{16,20},{20,16},{24,28},{28,24},{1,5},{5... | collective-permute-start | bytes 491528 | tf_op jit(solution)/shard_map/ppermute | solution.py:27
  166.5 25.0 %collective-permute-start.26 = (bf16[40,2048]{1,0:T(8,128)(2,1)S(1)}, bf16[40,2048]{1,0:T(8,128)(2,1)S(1)}, u32[]{:S(2)}, u32[]{:S(2)}) collective-permute-start(bf16[40,2048]{1,0:T(8,128)(2,1)S(1)} %get-tuple-element.49), channel_id=1, source_target_pairs={{0,8},{4,12},{8,0},{12,4},{16,24},{20,28},{24,16},{28,20},{1,9},{5... | collective-permute-start | bytes 491528 | tf_op jit(solution)/shard_map/ppermute | solution.py:27
  (28 other events, 308.0 us)
